TPU v7x, 256 devices: a 8x8x2 block of a 8x8x16 slice. The times are simulated.
256 devices in a mesh: grp: 2 (over z), ep: 64 (over y, x), tp: 2 (over core).
Axes of the slice: x: 8, y: 8, z: 2, core: 2. Of those that a mesh axis runs over, the one named last changes fastest.
The devices are a block of a 8x8x16 slice.
Arguments:
- tokens: bfloat16 [1024, 1536], P(('grp', 'ep')), parts along dimension 0, may hold values from -6 to 6
- norm_gain: float32 [1536], replicated, may hold values from 0.1 to 1.9
- routes: int32 [1024, 4], P(('grp', 'ep')), parts along dimension 0, may hold values from 0 to 63, all different within a row; in each aligned block of 8 rows (0 to 7, 8 to 15, ...) at most 2 rows name the same one
- route_weight: float32 [1024, 4], P(('grp', 'ep')), parts along dimension 0, may hold values from 0.1 to 1
- expert_gate: bfloat16 [64, 1536, 1536], P('ep', None, 'tp'), may hold values from -2 to 2
- expert_up: bfloat16 [64, 1536, 1536], P('ep', None, 'tp'), may hold values from -2 to 2
- expert_down: bfloat16 [64, 1536, 1536], P('ep', 'tp'), may hold values from -0.0390625 to 0.0390625
- dense_gate: bfloat16 [1536, 4096], P(None, ('ep', 'tp')), may hold values from -2 to 2
- dense_up: bfloat16 [1536, 4096], P(None, ('ep', 'tp')), may hold values from -2 to 2
- dense_down: bfloat16 [4096, 1536], P(('ep', 'tp')), may hold values from -0.0234375 to 0.0234375
- gate_vector: bfloat16 [4096], P(('ep', 'tp')), may hold values from -0.0234375 to 0.0234375
Outputs:
- mixed: bfloat16 [1024, 1536], P(('grp', 'ep'), 'tp'), parts along dimension 0
There are 2 independent parts, one for each index of `grp`. A program takes and returns all parts, laid end to end along the dimension named above; an argument that names none is the same for every part. Nothing has to cross between parts.
Inputs may be any that keep to these rules, and one draw needn't show every extreme that they name: `routes`: each token names 4 different experts. Within the rows of one index of ep (aligned blocks of 8 rows) no expert is named by more than 2 rows, a bound that some block reaches.
All inputs are finite; a program needn't handle non-finite values.
Results may differ from a plain program's by a relative error of at most 0.0077.
Values may be sent and summed in bfloat16 or wider, within the bound.
No kernel may reach another device: no remote copies, remote signals or barrier semaphores. Data moves between devices by JAX's collectives and lax.ppermute only.
A program may use at most 64 MiB of HBM per device.

v0:
```python
import functools
import math

import jax
import jax.numpy as jnp
from jax import lax
from jax.experimental import pallas as pl
from jax.experimental.pallas import tpu as pltpu
from jax.sharding import Mesh
from jax.sharding import PartitionSpec as P


EP = ("ep_0", "ep_1")
GRP_EP = ("grp", "ep_0", "ep_1")
EP_TP = ("ep_0", "ep_1", "tp")

clamp_limit = 7.0
sigmoid_slope = 1.702
norm_eps = 1e-06
capacity = 2
lane = 128
shape = ((0, 0), (0, 1), (0, -1), (1, 0))
classes = len(shape)

F32, BF16, I32 = jnp.float32, jnp.bfloat16, jnp.int32


def clamped_unit(gate_pre, up_pre):
    gated = jnp.minimum(gate_pre, clamp_limit)
    linear = jnp.clip(up_pre, -clamp_limit, clamp_limit)
    return (gated * jax.nn.sigmoid(sigmoid_slope * gated) * (linear + 1.0)).astype(BF16)


def dot(a, b):
    return lax.dot_general(a, b, (((1,), (0,)), ((), ())), preferred_element_type=F32)


def dot_nt(a, b):
    return lax.dot_general(a, b, (((1,), (1,)), ((), ())), preferred_element_type=F32)


def iota(dims, dim):
    return lax.broadcasted_iota(I32, dims, dim)


def swap_cores(value):
    return lax.ppermute(value, "tp", [(0, 1), (1, 0)])


def from_chip(value, down, across):
    high, wide = lax.axis_size("ep_0"), lax.axis_size("ep_1")
    pairs = [
        ((y + down) % high * wide + (x + across) % wide, y * wide + x)
        for y in range(high)
        for x in range(wide)
    ]
    return lax.ppermute(value, EP, pairs)


def class_of(chip, wide):
    return (chip % wide + 2 * (chip // wide)) % classes


def dispatch_kernel(wide, core, tokens_hbm, gain_hbm, routes_hbm, out, tokens, gain, routes, sems):
    copies = [
        pltpu.make_async_copy(src, dst, sems.at[n])
        for n, (src, dst) in enumerate(
            ((tokens_hbm, tokens), (routes_hbm, routes), (gain_hbm, gain))
        )
    ]
    for copy in copies:
        copy.start()
    tok_dev, width = tokens.shape
    half = width // 2
    top = routes.shape[0]
    ep_count = out.shape[0]
    slots = ep_count * capacity
    slot = iota((slots, tok_dev), 0)
    row = iota((slots, tok_dev), 1)
    expert = slot // capacity
    share = tok_dev // classes
    wanted = (row == class_of(expert, wide) * share + slot % capacity).astype(F32).astype(BF16)
    earlier = (iota((tok_dev, tok_dev), 0) < iota((tok_dev, tok_dev), 1)).astype(F32).astype(BF16)
    copies[1].wait()
    member = jnp.zeros((slots, tok_dev), F32)
    for k in range(top):
        member = jnp.where(routes[k : k + 1, :] == expert, 1.0, member)
    rank = dot(member.astype(BF16), earlier)
    taken = jnp.where(rank == (slot % capacity).astype(F32), member, 0.0).astype(BF16)
    copies[0].wait()
    copies[2].wait()
    values = tokens[...].astype(F32)
    inverse = lax.rsqrt(jnp.mean(values * values, axis=-1, keepdims=True) + norm_eps)
    low = core[0] == 0
    mine = jnp.where(low, values[:, :half], values[:, half:]) * inverse
    blocks = half // lane
    normed = []
    for n in range(blocks):
        scale = jnp.where(low, gain[n : n + 1, :], gain[blocks + n : blocks + n + 1, :])
        normed.append((mine[:, n * lane : (n + 1) * lane] * scale).astype(BF16))
    normed = jnp.concatenate(normed, axis=1)
    out[:, :, :half] = dot(taken, normed).astype(BF16).reshape(ep_count, capacity, half)
    out[:, :, half:] = dot(wanted, normed).astype(BF16).reshape(ep_count, capacity, half)


def pack_kernel(
    gate, up, down, vector_hbm, routes_hbm, weights_hbm, pack, combine, vector, routes, weights, sems
):
    units, width = gate.shape
    copies = [
        pltpu.make_async_copy(src, dst, sems.at[n])
        for n, (src, dst) in enumerate(
            (
                (vector_hbm, vector),
                (routes_hbm, routes),
                (weights_hbm, weights),
                (gate, pack.at[:, :width]),
                (up, pack.at[:, width : 2 * width]),
                (down, pack.at[:, 2 * width : 3 * width]),
            )
        )
    ]
    for copy in copies:
        copy.start()
    top, tok_dev = routes.shape
    slots = combine.shape[1]
    same = iota((units, units), 0) == iota((units, units), 1)
    first = (iota((units, lane), 1) == 0).astype(F32).astype(BF16)
    slot = iota((tok_dev, slots), 1)
    eye = iota((tok_dev, tok_dev), 0) == iota((tok_dev, tok_dev), 1)
    earlier = (iota((tok_dev, tok_dev), 1) < iota((tok_dev, tok_dev), 0)).astype(F32).astype(BF16)
    for copy in copies[:3]:
        copy.wait()
    spread = jnp.where(same, vector[...].astype(F32), 0.0).astype(BF16)
    pack[:, 3 * width :] = dot(spread, first).astype(BF16)
    member = jnp.zeros((tok_dev, slots), F32)
    weight = jnp.zeros((tok_dev, slots), F32)
    for k in range(top):
        named = jnp.sum(jnp.where(eye, routes[k : k + 1, :], 0), axis=1, keepdims=True)
        worth = jnp.sum(jnp.where(eye, weights[k : k + 1, :], 0.0), axis=1, keepdims=True)
        hit = named == slot // capacity
        member = jnp.where(hit, 1.0, member)
        weight = jnp.where(hit, worth, weight)
    rank = dot(earlier, member.astype(BF16))
    combine[...] = jnp.where(rank == (slot % capacity).astype(F32), weight, 0.0)
    for copy in copies[3:]:
        copy.wait()


def copy_all(pairs, sems):
    copies = [pltpu.make_async_copy(src, dst, sems.at[n]) for n, (src, dst) in enumerate(pairs)]
    for copy in copies:
        copy.start()
    return copies


def halves(core, half):
    at = pl.multiple_of(core[0] * half, half)
    to = pl.multiple_of((1 - core[0]) * half, half)
    return at, to


def fetch_kernel(core, gate_hbm, up_hbm, gate, up, sems):
    half = gate.shape[0]
    at, _ = halves(core, half)
    pairs = [(src.at[0, pl.ds(at, half), :], dst) for src, dst in ((gate_hbm, gate), (up_hbm, up))]
    for copy in copy_all(pairs, sems):
        copy.wait()


def own_kernel(
    core, mine, gate, up, gate_hbm, up_hbm, down_hbm, gate_pre, up_pre, gate_to, up_to, down, sems
):
    half = gate.shape[0]
    _, to = halves(core, half)
    copies = copy_all(
        (
            (gate_hbm.at[0, pl.ds(to, half), :], gate_to),
            (up_hbm.at[0, pl.ds(to, half), :], up_to),
            (down_hbm.at[0], down),
        ),
        sems,
    )
    x = mine[:, :, :half].reshape(-1, half)
    gate_pre[...] = dot(x, gate[...])
    up_pre[...] = dot(x, up[...])
    for copy in copies:
        copy.wait()


def rest_kernel(core, other, gate_pre, up_pre, gate, up, down, *refs):
    packs_hbm, (act, away, packs, sems) = refs[: classes - 1], refs[classes - 1 :]
    units = packs_hbm[0].shape[0]
    copies = copy_all(
        [(src, packs.at[n * units : (n + 1) * units, :]) for n, src in enumerate(packs_hbm)], sems
    )
    half = gate.shape[0]
    _, to = halves(core, half)
    y = other[:, :, :half].reshape(-1, half)
    value = clamped_unit(gate_pre[...] + dot(y, gate[...]), up_pre[...] + dot(y, up[...]))
    act[...] = value
    away[...] = dot(value, down[:, pl.ds(to, half)]).astype(BF16)
    for copy in copies:
        copy.wait()


def rows(packs, start, size):
    return jnp.concatenate([p[:, pl.ds(start, size)] for p in packs], axis=0)


def dense_kernel(core, mine, other, pack, neighbours, hidden, away):
    packs = (pack, neighbours)
    half = mine.shape[2] // 2
    width = 2 * half
    at, to = halves(core, half)
    x = mine[:, :, half:].reshape(-1, half)
    y = other[:, :, half:].reshape(-1, half)
    gate_pre = dot_nt(x, rows(packs, at, half)) + dot_nt(y, rows(packs, to, half))
    up_pre = dot_nt(x, rows(packs, width + at, half)) + dot_nt(y, rows(packs, width + to, half))
    value = clamped_unit(gate_pre, up_pre)
    hidden[...] = value
    away[:, :half] = dot(value, rows(packs, 2 * width + to, half)).astype(BF16)
    away[:, half:] = dot(value, rows(packs, 3 * width, lane)).astype(BF16)


def here_kernel(core, act, hidden, down, pack, neighbours, out):
    packs = (pack, neighbours)
    half = down.shape[1] // 2
    width = 2 * half
    at, _ = halves(core, half)
    out[:, :half] = dot(act[...], down[:, pl.ds(at, half)]).astype(BF16)
    value = hidden[...]
    out[:, half:width] = dot(value, rows(packs, 2 * width + at, half)).astype(BF16)
    out[:, width:] = dot(value, rows(packs, 3 * width, lane)).astype(BF16)


def join_kernel(here, expert_away, dense_away, out):
    half = expert_away.shape[1]
    shape3 = out.shape[:2] + (-1,)
    mine = here[...].astype(F32)
    expert = (mine[:, :half] + expert_away[...].astype(F32)).astype(BF16)
    dense = (mine[:, half:] + dense_away[...].astype(F32)).astype(BF16)
    out[:, :, :half] = expert.reshape(shape3)
    out[:, :, half:] = dense.reshape(shape3)


def mix_kernel(wide, returned, combine, out):
    tok_dev, half = out.shape
    slots = returned.shape[0] * returned.shape[1]
    slot = iota((tok_dev, slots), 1)
    share = tok_dev // classes
    owner = class_of(slot // capacity, wide) * share + slot % capacity
    wanted = (iota((tok_dev, slots), 0) == owner).astype(F32).astype(BF16)
    dense_out = dot(wanted, returned[:, :, half : 2 * half].reshape(slots, half))
    gate_logit = dot(wanted, returned[:, :, 2 * half :].reshape(slots, lane))[:, :1]
    first = combine[...].astype(BF16)
    rest = combine[...] - first.astype(F32)
    second = rest.astype(BF16)
    third = (rest - second.astype(F32)).astype(BF16)
    expert_rows = returned[:, :, :half].reshape(slots, half)
    expert_mix = dot(first, expert_rows) + (dot(second, expert_rows) + dot(third, expert_rows))
    out[...] = (jax.nn.sigmoid(gate_logit) * dense_out + expert_mix).astype(BF16)


def call(kernel, outs, *operands, inside=0, scratch=(), room=8 * 2**20):
    specs, placed = [], []
    for n, operand in enumerate(operands):
        if n >= len(operands) - inside:
            specs.append(pl.BlockSpec(memory_space=pl.ANY))
            placed.append(pltpu.with_memory_space_constraint(operand, pltpu.HBM))
        elif operand.dtype == I32 and operand.ndim == 1:
            specs.append(pl.BlockSpec(memory_space=pltpu.SMEM))
            placed.append(operand)
        else:
            specs.append(pl.BlockSpec(memory_space=pltpu.VMEM))
            placed.append(operand)
    many = isinstance(outs, list)
    spec = pl.BlockSpec(memory_space=pltpu.VMEM)
    return pl.pallas_call(
        kernel,
        out_shape=outs,
        in_specs=specs,
        out_specs=[spec] * len(outs) if many else spec,
        scratch_shapes=list(scratch),
        cost_estimate=pl.CostEstimate(flops=10**9, transcendentals=0, bytes_accessed=0),
        compiler_params=pltpu.CompilerParams(vmem_limit_bytes=room),
    )(*placed)


def per_device(
    tokens,
    norm_gain,
    routes,
    route_weight,
    expert_gate,
    expert_up,
    expert_down,
    dense_gate,
    dense_up,
    dense_down,
    gate_vector,
):
    tok_dev, width = tokens.shape
    top = routes.shape[1]
    half = width // lax.axis_size("tp")
    ep_count = lax.axis_size(EP)
    wide = lax.axis_size("ep_1")
    slots = ep_count * capacity
    units, hidden_units = dense_down.shape[0], expert_down.shape[1]
    core = lax.axis_index("tp").reshape(1)

    def exchange(rows):
        return lax.all_to_all(rows, EP, split_axis=0, concat_axis=0, tiled=True)

    def out(*dims, dtype=BF16):
        return pltpu.VMEM(dims, dtype)

    outgoing = call(
        functools.partial(dispatch_kernel, wide),
        out(ep_count, capacity, width),
        core,
        tokens,
        norm_gain.reshape(-1, lane),
        routes.T,
        inside=3,
        scratch=(
            pltpu.VMEM((tok_dev, width), BF16),
            pltpu.VMEM((width // lane, lane), F32),
            pltpu.VMEM((top, tok_dev), I32),
            pltpu.SemaphoreType.DMA((3,)),
        ),
    )
    mine = exchange(outgoing)
    pack, combine = call(
        pack_kernel,
        [out(units, 3 * width + lane), out(tok_dev, slots, dtype=F32)],
        dense_gate.T,
        dense_up.T,
        dense_down,
        gate_vector.reshape(1, -1),
        routes.T,
        route_weight.T,
        inside=6,
        scratch=(
            pltpu.VMEM((1, units), BF16),
            pltpu.VMEM((top, tok_dev), I32),
            pltpu.VMEM((top, tok_dev), F32),
            pltpu.SemaphoreType.DMA((6,)),
        ),
    )
    packs = []
    for offset in shape[1:]:
        packs.append(from_chip(pack, *offset))
    dma = pltpu.SemaphoreType.DMA
    gate, up = call(
        fetch_kernel,
        [out(half, hidden_units)] * 2,
        core,
        expert_gate,
        expert_up,
        inside=2,
        scratch=(dma((2,)),),
    )
    other = swap_cores(mine)
    gate_pre, up_pre, gate, up, down = call(
        own_kernel,
        [out(slots, hidden_units, dtype=F32)] * 2
        + [out(half, hidden_units)] * 2
        + [out(hidden_units, width)],
        core,
        mine,
        gate,
        up,
        expert_gate,
        expert_up,
        expert_down,
        inside=3,
        scratch=(dma((3,)),),
    )
    act, expert_away, neighbours = call(
        rest_kernel,
        [out(slots, hidden_units), out(slots, half), out((classes - 1) * units, 3 * width + lane)],
        core,
        other,
        gate_pre,
        up_pre,
        gate,
        up,
        down,
        *packs,
        inside=classes - 1,
        scratch=(dma((classes - 1,)),),
    )
    expert_away = swap_cores(expert_away)
    hidden, dense_away = call(
        dense_kernel,
        [out(slots, classes * units), out(slots, half + lane)],
        core,
        mine,
        other,
        pack,
        neighbours,
    )
    dense_away = swap_cores(dense_away)
    here = call(here_kernel, out(slots, width + lane), core, act, hidden, down, pack, neighbours)
    terms = call(join_kernel, out(ep_count, capacity, width + lane), here, expert_away, dense_away)
    returned = exchange(terms)
    return call(
        functools.partial(mix_kernel, wide),
        jax.ShapeDtypeStruct((tok_dev, half), BF16),
        returned,
        combine,
    )


def solution(mesh):
    side = math.isqrt(mesh.shape["ep"])
    split = Mesh(
        mesh.devices.reshape(mesh.shape["grp"], side, side, mesh.shape["tp"]),
        ("grp", "ep_0", "ep_1", "tp"),
    )
    placed = (
        P(GRP_EP, None),
        P(),
        P(GRP_EP, None),
        P(GRP_EP, None),
        P(EP, None, "tp"),
        P(EP, None, "tp"),
        P(EP, "tp", None),
        P(None, EP_TP),
        P(None, EP_TP),
        P(EP_TP, None),
        P(EP_TP),
    )

    return jax.shard_map(
        per_device, mesh=split, in_specs=placed, out_specs=P(GRP_EP, "tp"), check_vma=False
    )
```

profile of v0, /device:TPU:514, one launch (start us, length us, event | category | flops | bytes accessed | tf_op | source)
XLA Modules:
  0.0 81.9 jit_solution(5709969880871709679)
XLA Ops:
  0.0 1.2 %shard_map.109 = bf16[64,2,1536]{2,1,0:T(2,128)(2,1)S(1)} custom-call(s32[1]{0:T(128)} %bitcast.core, bf16[8,1536]{1,0:T(8,128)(2,1)} %tokens_hbm.1, f32[12,128]{1,0:T(8,128)} %bitcast.9, s32[4,8]{1,0:T(4,128)} %bitcast.10), custom_call_target="tpu_custom_call" | custom-call | flops 1000000000 | tf_op jit(solution)/shard_map/pallas_call | solution.py:279
  1.2 37.4 %all_to_all.10.mine = bf16[64,2,1536]{2,1,0:T(2,128)(2,1)S(1)} all-to-all(bf16[64,2,1536]{2,1,0:T(2,128)(2,1)S(1)} %shard_map.109), channel_id=1, replica_groups=mesh['grp'=2,'ep_0'=8,'ep_1'=8,'tp'=2] {'ep_0','ep_1'}, dimensions={0} | all-to-all | bytes 786432 | tf_op jit(solution)/shard_map/all_to_all | solution.py:313
  38.6 0.0 collective-permute-start
  38.6 1.1 %shard_map.112 = (bf16[32,4736]{1,0:T(8,128)(2,1)S(1)}, f32[8,128]{1,0:T(8,128)S(1)}) custom-call(bf16[32,1536]{1,0:T(8,128)(2,1)} %bitcast.7, bf16[32,1536]{1,0:T(8,128)(2,1)} %bitcast.8, bf16[32,1536]{1,0:T(8,128)(2,1)} %down.1, bf16[1,32]{1,0:T(2,128)(2,1)} %bitcast.13, s32[4,8]{1,0:T(4,128)} %bitcast.11, f32[4,8]{1,0:T(4,128)} %bitcast.12), custom_call_target="tpu_custom_call" | custom-call | flops 1000000000 | tf_op jit(solution)/shard_map/pallas_call | solution.py:279
  39.7 1.0 %collective-permute-start.1 = (bf16[32,4736]{1,0:T(8,128)(2,1)S(1)}, bf16[32,4736]{1,0:T(8,128)(2,1)S(1)}, u32[]{:S(2)}, u32[]{:S(2)}) collective-permute-start(bf16[32,4736]{1,0:T(8,128)(2,1)S(1)} %get-tuple-element.26.pack), channel_id=1, source_target_pairs={{2,0},{4,2},{6,4},{8,6},{10,8},{12,10},{14,12},{0,14},{18,16},{20,... | collective-permute-start | bytes 909320 | tf_op jit(solution)/shard_map/ppermute | solution.py:57
  40.7 1.2 %collective-permute-start.2 = (bf16[32,4736]{1,0:T(8,128)(2,1)S(1)}, bf16[32,4736]{1,0:T(8,128)(2,1)S(1)}, u32[]{:S(2)}, u32[]{:S(2)}) collective-permute-start(bf16[32,4736]{1,0:T(8,128)(2,1)S(1)} %get-tuple-element.26.pack), channel_id=1, source_target_pairs={{14,0},{0,2},{2,4},{4,6},{6,8},{8,10},{10,12},{12,14},{30,16},{16,... | collective-permute-start | bytes 909320 | tf_op jit(solution)/shard_map/ppermute | solution.py:57
  41.9 0.4 collective-permute-start.3
  42.3 1.6 %shard_map.110 = (bf16[768,768]{1,0:T(8,128)(2,1)S(1)}, bf16[768,768]{1,0:T(8,128)(2,1)S(1)}) custom-call(s32[1]{0:T(128)} %bitcast.core, bf16[1,1536,768]{2,1,0:T(8,128)(2,1)} %gate_hbm.3, bf16[1,1536,768]{2,1,0:T(8,128)(2,1)} %up_hbm.3), custom_call_target="tpu_custom_call" | custom-call | flops 1000000000 | tf_op jit(solution)/shard_map/pallas_call | solution.py:279
  43.9 2.8 %shard_map.111 = (f32[128,768]{1,0:T(8,128)S(1)}, f32[128,768]{1,0:T(8,128)S(1)}, bf16[768,768]{1,0:T(8,128)(2,1)S(1)}, bf16[768,768]{1,0:T(8,128)(2,1)S(1)}, bf16[768,1536]{1,0:T(8,128)(2,1)S(1)}) custom-call(s32[1]{0:T(128)} %bitcast.core, bf16[64,2,1536]{2,1,0:T(2,128)(2,1)S(1)} %all_to_all.10.mine, bf16[768,768]{1,0:T(8,128)(2,1)S(1)} %get-tuple-element.19.gate, ...), custom_call_target="tpu_custom_call" | custom-call | flops 1000000000 | tf_op jit(solution)/shard_map/pallas_call | solution.py:279
  46.7 2.7 %collective-permute-done.1.refs_0_ = bf16[32,4736]{1,0:T(8,128)(2,1)S(1)} collective-permute-done((bf16[32,4736]{1,0:T(8,128)(2,1)S(1)}, bf16[32,4736]{1,0:T(8,128)(2,1)S(1)}, u32[]{:S(2)}, u32[]{:S(2)}) %collective-permute-start.1) | collective-permute-done | bytes 303136 | tf_op jit(solution)/shard_map/ppermute | solution.py:57
  49.4 0.0 copy-start
  49.5 0.6 collective-permute-done.2.refs_1_
  50.0 0.0 copy-start.1
  50.0 0.9 %collective-permute-done.3.refs_2_ = bf16[32,4736]{1,0:T(8,128)(2,1)S(1)} collective-permute-done((bf16[32,4736]{1,0:T(8,128)(2,1)S(1)}, bf16[32,4736]{1,0:T(8,128)(2,1)S(1)}, u32[]{:S(2)}, u32[]{:S(2)}) %collective-permute-start.3) | collective-permute-done | bytes 303136 | tf_op jit(solution)/shard_map/ppermute | solution.py:57
  50.9 0.0 copy-start.2
  50.9 0.0 collective-permute-done.other
  50.9 0.0 copy-done
  50.9 0.0 copy-done.1
  50.9 0.7 copy-done.2
  51.6 1.7 %shard_map.113 = (bf16[128,768]{1,0:T(8,128)(2,1)S(1)}, bf16[128,768]{1,0:T(8,128)(2,1)S(1)}, bf16[96,4736]{1,0:T(8,128)(2,1)S(1)}) custom-call(s32[1]{0:T(128)} %bitcast.core, bf16[64,2,1536]{2,1,0:T(2,128)(2,1)S(1)} %collective-permute-done.other, f32[128,768]{1,0:T(8,128)S(1)} %get-tuple-element.21.gate_pre, f32[128,768]{1,0:T(8,128)S(1)} %get-tuple-element.22.up_pre, ...), custom_call_target="tpu_custom_call" | custom-call | flops 1000000000 | tf_op jit(solution)/shard_map/pallas_call | solution.py:279
  53.3 0.6 shard_map.114
  53.9 0.1 collective-permute-start.5
  54.0 0.5 collective-permute-start.4
  54.5 0.4 shard_map.115.here
  54.9 0.9 %collective-permute-done.4.expert_away = bf16[128,768]{1,0:T(8,128)(2,1)S(1)} collective-permute-done((bf16[128,768]{1,0:T(8,128)(2,1)S(1)}, bf16[128,768]{1,0:T(8,128)(2,1)S(1)}, u32[]{:S(2)}, u32[]{:S(2)}) %collective-permute-start.4) | collective-permute-done | bytes 196640 | tf_op jit(solution)/shard_map/ppermute | solution.py:47
  55.8 0.0 collective-permute-done.5.dense_away
  55.8 0.2 shard_map.116
  55.9 25.1 %all_to_all.11.returned = bf16[64,2,1664]{2,1,0:T(2,128)(2,1)S(1)} all-to-all(bf16[64,2,1664]{2,1,0:T(2,128)(2,1)S(1)} %shard_map.116), channel_id=1, replica_groups=mesh['grp'=2,'ep_0'=8,'ep_1'=8,'tp'=2] {'ep_0','ep_1'}, dimensions={0} | all-to-all | bytes 851968 | tf_op jit(solution)/shard_map/all_to_all | solution.py:313
  81.0 0.9 %shard_map.117 = bf16[8,768]{1,0:T(8,128)(2,1)} custom-call(bf16[64,2,1664]{2,1,0:T(2,128)(2,1)S(1)} %all_to_all.11.returned, f32[8,128]{1,0:T(8,128)S(1)} %get-tuple-element.32.combine), custom_call_target="tpu_custom_call" | custom-call | flops 1000000000 | tf_op jit(solution)/shard_map/pallas_call | solution.py:279
Async XLA Ops:
  38.6 12.3 %collective-permute-start = (bf16[64,2,1536]{2,1,0:T(2,128)(2,1)S(1)}, bf16[64,2,1536]{2,1,0:T(2,128)(2,1)S(1)}, u32[]{:S(2)}, u32[]{:S(2)}) collective-permute-start(bf16[64,2,1536]{2,1,0:T(2,128)(2,1)S(1)} %all_to_all.10.mine), channel_id=1, source_target_pairs={{0,1},{1,0},{2,3},{3,2},{4,5},{5,4},{6,7},{7,6},{8,9},{9,8},{10,11... | collective-permute-start | bytes 1179656 | tf_op jit(solution)/shard_map/ppermute | solution.py:47
  39.7 9.7 %collective-permute-start.1 = (bf16[32,4736]{1,0:T(8,128)(2,1)S(1)}, bf16[32,4736]{1,0:T(8,128)(2,1)S(1)}, u32[]{:S(2)}, u32[]{:S(2)}) collective-permute-start(bf16[32,4736]{1,0:T(8,128)(2,1)S(1)} %get-tuple-element.26.pack), channel_id=1, source_target_pairs={{2,0},{4,2},{6,4},{8,6},{10,8},{12,10},{14,12},{0,14},{18,16},{20,... | collective-permute-start | bytes 909320 | tf_op jit(solution)/shard_map/ppermute | solution.py:57
  40.7 9.3 %collective-permute-start.2 = (bf16[32,4736]{1,0:T(8,128)(2,1)S(1)}, bf16[32,4736]{1,0:T(8,128)(2,1)S(1)}, u32[]{:S(2)}, u32[]{:S(2)}) collective-permute-start(bf16[32,4736]{1,0:T(8,128)(2,1)S(1)} %get-tuple-element.26.pack), channel_id=1, source_target_pairs={{14,0},{0,2},{2,4},{4,6},{6,8},{8,10},{10,12},{12,14},{30,16},{16,... | collective-permute-start | bytes 909320 | tf_op jit(solution)/shard_map/ppermute | solution.py:57
  41.9 9.0 %collective-permute-start.3 = (bf16[32,4736]{1,0:T(8,128)(2,1)S(1)}, bf16[32,4736]{1,0:T(8,128)(2,1)S(1)}, u32[]{:S(2)}, u32[]{:S(2)}) collective-permute-start(bf16[32,4736]{1,0:T(8,128)(2,1)S(1)} %get-tuple-element.26.pack), channel_id=1, source_target_pairs={{16,0},{18,2},{20,4},{22,6},{24,8},{26,10},{28,12},{30,14},{32,16}... | collective-permute-start | bytes 909320 | tf_op jit(solution)/shard_map/ppermute | solution.py:57
  49.4 1.5 %copy-start = (bf16[32,4736]{1,0:T(8,128)(2,1)}, bf16[32,4736]{1,0:T(8,128)(2,1)S(1)}, u32[]{:S(2)}) copy-start(bf16[32,4736]{1,0:T(8,128)(2,1)S(1)} %collective-permute-done.1.refs_0_) | copy-start | bytes 909316
  50.0 0.9 %copy-start.1 = (bf16[32,4736]{1,0:T(8,128)(2,1)}, bf16[32,4736]{1,0:T(8,128)(2,1)S(1)}, u32[]{:S(2)}) copy-start(bf16[32,4736]{1,0:T(8,128)(2,1)S(1)} %collective-permute-done.2.refs_1_) | copy-start | bytes 909316
  50.9 0.7 copy-start.2
  53.9 1.9 %collective-permute-start.5 = (bf16[128,896]{1,0:T(8,128)(2,1)S(1)}, bf16[128,896]{1,0:T(8,128)(2,1)S(1)}, u32[]{:S(2)}, u32[]{:S(2)}) collective-permute-start(bf16[128,896]{1,0:T(8,128)(2,1)S(1)} %get-tuple-element.31), channel_id=1, source_target_pairs={{0,1},{1,0},{2,3},{3,2},{4,5},{5,4},{6,7},{7,6},{8,9},{9,8},{10,11... | collective-permute-start | bytes 688136 | tf_op jit(solution)/shard_map/ppermute | solution.py:47
  54.0 1.7 %collective-permute-start.4 = (bf16[128,768]{1,0:T(8,128)(2,1)S(1)}, bf16[128,768]{1,0:T(8,128)(2,1)S(1)}, u32[]{:S(2)}, u32[]{:S(2)}) collective-permute-start(bf16[128,768]{1,0:T(8,128)(2,1)S(1)} %get-tuple-element.30), channel_id=1, source_target_pairs={{0,1},{1,0},{2,3},{3,2},{4,5},{5,4},{6,7},{7,6},{8,9},{9,8},{10,11... | collective-permute-start | bytes 589832 | tf_op jit(solution)/shard_map/ppermute | solution.py:47
where the time goes:
time: 82.2 us; the launch traced here: 81.9 us
  blocking collectives  62.5 us (76%)
  Pallas kernels  10.3 us (13%)
  waiting for transfers between devices  5.08 us (6%)
  starting transfers between devices  3.18 us (4%)
    all_to_all x2, blocking collectives, exchange(): return lax.all_to_all(rows, EP, split_axis=0, concat_axis=0, tiled=True)  62.5 us
    pallas_call x9, Pallas kernels, call(): pl.pallas_call(kernel, out_shape=outs, in_specs=specs, out_specs=[spec] *...  10.3 us
    ppermute x3, waiting for transfers between devices, from_chip(): return lax.ppermute(value, EP, pairs)  4.2 us
    ppermute x3, starting transfers between devices, from_chip(): return lax.ppermute(value, EP, pairs)  2.55 us
  transfers between devices with their start and end apart: 6, of which 4 were waited for; matrix products, arithmetic and copies ran while one was open for 0% of the time, Pallas kernels for 7%

commit v1 on v0

--- a/solution.py
+++ b/solution.py
@@ -61,34 +61,65 @@
     return (chip % wide + 2 * (chip // wide)) % classes
 
 
-def dispatch_kernel(wide, core, tokens_hbm, gain_hbm, routes_hbm, out, tokens, gain, routes, sems):
-    copies = [
-        pltpu.make_async_copy(src, dst, sems.at[n])
-        for n, (src, dst) in enumerate(
-            ((tokens_hbm, tokens), (routes_hbm, routes), (gain_hbm, gain))
-        )
-    ]
+def copy_all(pairs, sems):
+    copies = [pltpu.make_async_copy(src, dst, sems.at[n]) for n, (src, dst) in enumerate(pairs)]
     for copy in copies:
         copy.start()
+    return copies
+
+
+def first_kernel(
+    wide,
+    core,
+    tokens_hbm,
+    routes_hbm,
+    gain_hbm,
+    vector_hbm,
+    gate_hbm,
+    up_hbm,
+    down_hbm,
+    out,
+    pack,
+    tokens,
+    routes,
+    gain,
+    vector,
+    sems,
+):
     tok_dev, width = tokens.shape
+    copies = copy_all(
+        (
+            (routes_hbm, routes),
+            (tokens_hbm, tokens),
+            (gain_hbm, gain),
+            (vector_hbm, vector),
+            (gate_hbm, pack.at[:, :width]),
+            (up_hbm, pack.at[:, width : 2 * width]),
+            (down_hbm, pack.at[:, 2 * width : 3 * width]),
+        ),
+        sems,
+    )
     half = width // 2
     top = routes.shape[0]
     ep_count = out.shape[0]
     slots = ep_count * capacity
+    units = pack.shape[0]
     slot = iota((slots, tok_dev), 0)
     row = iota((slots, tok_dev), 1)
     expert = slot // capacity
     share = tok_dev // classes
     wanted = (row == class_of(expert, wide) * share + slot % capacity).astype(F32).astype(BF16)
     earlier = (iota((tok_dev, tok_dev), 0) < iota((tok_dev, tok_dev), 1)).astype(F32).astype(BF16)
-    copies[1].wait()
+    same = iota((units, units), 0) == iota((units, units), 1)
+    lead = (iota((units, lane), 1) == 0).astype(F32).astype(BF16)
+    copies[0].wait()
     member = jnp.zeros((slots, tok_dev), F32)
     for k in range(top):
         member = jnp.where(routes[k : k + 1, :] == expert, 1.0, member)
     rank = dot(member.astype(BF16), earlier)
     taken = jnp.where(rank == (slot % capacity).astype(F32), member, 0.0).astype(BF16)
-    copies[0].wait()
-    copies[2].wait()
+    for copy in copies[1:4]:
+        copy.wait()
     values = tokens[...].astype(F32)
     inverse = lax.rsqrt(jnp.mean(values * values, axis=-1, keepdims=True) + norm_eps)
     low = core[0] == 0
@@ -99,40 +130,20 @@
         scale = jnp.where(low, gain[n : n + 1, :], gain[blocks + n : blocks + n + 1, :])
         normed.append((mine[:, n * lane : (n + 1) * lane] * scale).astype(BF16))
     normed = jnp.concatenate(normed, axis=1)
+    spread = jnp.where(same, vector[...].astype(F32), 0.0).astype(BF16)
+    pack[:, 3 * width :] = dot(spread, lead).astype(BF16)
     out[:, :, :half] = dot(taken, normed).astype(BF16).reshape(ep_count, capacity, half)
     out[:, :, half:] = dot(wanted, normed).astype(BF16).reshape(ep_count, capacity, half)
-
-
-def pack_kernel(
-    gate, up, down, vector_hbm, routes_hbm, weights_hbm, pack, combine, vector, routes, weights, sems
-):
-    units, width = gate.shape
-    copies = [
-        pltpu.make_async_copy(src, dst, sems.at[n])
-        for n, (src, dst) in enumerate(
-            (
-                (vector_hbm, vector),
-                (routes_hbm, routes),
-                (weights_hbm, weights),
-                (gate, pack.at[:, :width]),
-                (up, pack.at[:, width : 2 * width]),
-                (down, pack.at[:, 2 * width : 3 * width]),
-            )
-        )
-    ]
-    for copy in copies:
-        copy.start()
+    for copy in copies[4:]:
+        copy.wait()
+
+
+def weigh(routes, weights, combine):
     top, tok_dev = routes.shape
     slots = combine.shape[1]
-    same = iota((units, units), 0) == iota((units, units), 1)
-    first = (iota((units, lane), 1) == 0).astype(F32).astype(BF16)
     slot = iota((tok_dev, slots), 1)
     eye = iota((tok_dev, tok_dev), 0) == iota((tok_dev, tok_dev), 1)
     earlier = (iota((tok_dev, tok_dev), 1) < iota((tok_dev, tok_dev), 0)).astype(F32).astype(BF16)
-    for copy in copies[:3]:
-        copy.wait()
-    spread = jnp.where(same, vector[...].astype(F32), 0.0).astype(BF16)
-    pack[:, 3 * width :] = dot(spread, first).astype(BF16)
     member = jnp.zeros((tok_dev, slots), F32)
     weight = jnp.zeros((tok_dev, slots), F32)
     for k in range(top):
@@ -143,15 +154,6 @@
         weight = jnp.where(hit, worth, weight)
     rank = dot(earlier, member.astype(BF16))
     combine[...] = jnp.where(rank == (slot % capacity).astype(F32), weight, 0.0)
-    for copy in copies[3:]:
-        copy.wait()
-
-
-def copy_all(pairs, sems):
-    copies = [pltpu.make_async_copy(src, dst, sems.at[n]) for n, (src, dst) in enumerate(pairs)]
-    for copy in copies:
-        copy.start()
-    return copies
 
 
 def halves(core, half):
@@ -160,56 +162,60 @@
     return at, to
 
 
-def fetch_kernel(core, gate_hbm, up_hbm, gate, up, sems):
-    half = gate.shape[0]
-    at, _ = halves(core, half)
-    pairs = [(src.at[0, pl.ds(at, half), :], dst) for src, dst in ((gate_hbm, gate), (up_hbm, up))]
-    for copy in copy_all(pairs, sems):
-        copy.wait()
-
-
 def own_kernel(
-    core, mine, gate, up, gate_hbm, up_hbm, down_hbm, gate_pre, up_pre, gate_to, up_to, down, sems
+    core,
+    mine,
+    gate,
+    up_hbm,
+    routes_hbm,
+    weights_hbm,
+    gate_pre,
+    up_pre,
+    up,
+    combine,
+    routes,
+    weights,
+    sems,
 ):
-    half = gate.shape[0]
-    _, to = halves(core, half)
+    half = mine.shape[2] // 2
+    at, to = halves(core, half)
     copies = copy_all(
         (
-            (gate_hbm.at[0, pl.ds(to, half), :], gate_to),
-            (up_hbm.at[0, pl.ds(to, half), :], up_to),
-            (down_hbm.at[0], down),
+            (up_hbm.at[0, pl.ds(at, half), :], up.at[pl.ds(at, half), :]),
+            (routes_hbm, routes),
+            (weights_hbm, weights),
+            (up_hbm.at[0, pl.ds(to, half), :], up.at[pl.ds(to, half), :]),
         ),
         sems,
     )
     x = mine[:, :, :half].reshape(-1, half)
-    gate_pre[...] = dot(x, gate[...])
-    up_pre[...] = dot(x, up[...])
-    for copy in copies:
-        copy.wait()
-
-
-def rest_kernel(core, other, gate_pre, up_pre, gate, up, down, *refs):
-    packs_hbm, (act, away, packs, sems) = refs[: classes - 1], refs[classes - 1 :]
-    units = packs_hbm[0].shape[0]
-    copies = copy_all(
-        [(src, packs.at[n * units : (n + 1) * units, :]) for n, src in enumerate(packs_hbm)], sems
-    )
-    half = gate.shape[0]
+    gate_pre[...] = dot(x, gate[0, pl.ds(at, half), :])
+    copies[1].wait()
+    copies[2].wait()
+    weigh(routes, weights, combine)
+    copies[0].wait()
+    up_pre[...] = dot(x, up[pl.ds(at, half), :])
+    copies[3].wait()
+
+
+def rest_kernel(core, other, gate_pre, up_pre, gate, up, down, act, away):
+    half = other.shape[2] // 2
     _, to = halves(core, half)
     y = other[:, :, :half].reshape(-1, half)
-    value = clamped_unit(gate_pre[...] + dot(y, gate[...]), up_pre[...] + dot(y, up[...]))
+    value = clamped_unit(
+        gate_pre[...] + dot(y, gate[0, pl.ds(to, half), :]),
+        up_pre[...] + dot(y, up[pl.ds(to, half), :]),
+    )
     act[...] = value
-    away[...] = dot(value, down[:, pl.ds(to, half)]).astype(BF16)
-    for copy in copies:
-        copy.wait()
+    away[...] = dot(value, down[0, :, pl.ds(to, half)]).astype(BF16)
 
 
 def rows(packs, start, size):
     return jnp.concatenate([p[:, pl.ds(start, size)] for p in packs], axis=0)
 
 
-def dense_kernel(core, mine, other, pack, neighbours, hidden, away):
-    packs = (pack, neighbours)
+def dense_kernel(core, mine, other, *refs):
+    packs, (hidden, away) = refs[:classes], refs[classes:]
     half = mine.shape[2] // 2
     width = 2 * half
     at, to = halves(core, half)
@@ -223,12 +229,12 @@
     away[:, half:] = dot(value, rows(packs, 3 * width, lane)).astype(BF16)
 
 
-def here_kernel(core, act, hidden, down, pack, neighbours, out):
-    packs = (pack, neighbours)
-    half = down.shape[1] // 2
+def here_kernel(core, act, hidden, down, *refs):
+    packs, out = refs[:classes], refs[classes]
+    half = down.shape[2] // 2
     width = 2 * half
     at, _ = halves(core, half)
-    out[:, :half] = dot(act[...], down[:, pl.ds(at, half)]).astype(BF16)
+    out[:, :half] = dot(act[...], down[0, :, pl.ds(at, half)]).astype(BF16)
     value = hidden[...]
     out[:, half:width] = dot(value, rows(packs, 2 * width + at, half)).astype(BF16)
     out[:, width:] = dot(value, rows(packs, 3 * width, lane)).astype(BF16)
@@ -315,71 +321,55 @@
     def out(*dims, dtype=BF16):
         return pltpu.VMEM(dims, dtype)
 
-    outgoing = call(
-        functools.partial(dispatch_kernel, wide),
-        out(ep_count, capacity, width),
+    dma = pltpu.SemaphoreType.DMA
+    outgoing, pack = call(
+        functools.partial(first_kernel, wide),
+        [out(ep_count, capacity, width), out(units, 3 * width + lane)],
         core,
         tokens,
+        routes.T,
         norm_gain.reshape(-1, lane),
-        routes.T,
-        inside=3,
-        scratch=(
-            pltpu.VMEM((tok_dev, width), BF16),
-            pltpu.VMEM((width // lane, lane), F32),
-            pltpu.VMEM((top, tok_dev), I32),
-            pltpu.SemaphoreType.DMA((3,)),
-        ),
-    )
-    mine = exchange(outgoing)
-    pack, combine = call(
-        pack_kernel,
-        [out(units, 3 * width + lane), out(tok_dev, slots, dtype=F32)],
+        gate_vector.reshape(1, -1),
         dense_gate.T,
         dense_up.T,
         dense_down,
-        gate_vector.reshape(1, -1),
-        routes.T,
-        route_weight.T,
-        inside=6,
+        inside=7,
         scratch=(
+            pltpu.VMEM((tok_dev, width), BF16),
+            pltpu.VMEM((top, tok_dev), I32),
+            pltpu.VMEM((width // lane, lane), F32),
             pltpu.VMEM((1, units), BF16),
-            pltpu.VMEM((top, tok_dev), I32),
-            pltpu.VMEM((top, tok_dev), F32),
-            pltpu.SemaphoreType.DMA((6,)),
+            dma((7,)),
         ),
     )
-    packs = []
+    packs = [pack]
     for offset in shape[1:]:
         packs.append(from_chip(pack, *offset))
-    dma = pltpu.SemaphoreType.DMA
-    gate, up = call(
-        fetch_kernel,
-        [out(half, hidden_units)] * 2,
-        core,
-        expert_gate,
-        expert_up,
-        inside=2,
-        scratch=(dma((2,)),),
+    mine = exchange(outgoing)
+    gate, down = (
+        pltpu.with_memory_space_constraint(w, pltpu.VMEM) for w in (expert_gate, expert_down)
     )
     other = swap_cores(mine)
-    gate_pre, up_pre, gate, up, down = call(
+    gate_pre, up_pre, up, combine = call(
         own_kernel,
         [out(slots, hidden_units, dtype=F32)] * 2
-        + [out(half, hidden_units)] * 2
-        + [out(hidden_units, width)],
+        + [out(width, hidden_units), out(tok_dev, slots, dtype=F32)],
         core,
         mine,
         gate,
-        up,
-        expert_gate,
         expert_up,
-        expert_down,
+        routes.T,
+        route_weight.T,
         inside=3,
-        scratch=(dma((3,)),),
-    )
-    act, expert_away, neighbours = call(
+        scratch=(
+            pltpu.VMEM((top, tok_dev), I32),
+            pltpu.VMEM((top, tok_dev), F32),
+            dma((4,)),
+        ),
+    )
+    act, expert_away = call(
         rest_kernel,
-        [out(slots, hidden_units), out(slots, half), out((classes - 1) * units, 3 * width + lane)],
+        [out(slots, hidden_units), out(slots, half)],
         core,
         other,
         gate_pre,
@@ -387,9 +377,6 @@
         gate,
         up,
         down,
-        *packs,
-        inside=classes - 1,
-        scratch=(dma((classes - 1,)),),
     )
     expert_away = swap_cores(expert_away)
     hidden, dense_away = call(
@@ -398,11 +385,10 @@
         core,
         mine,
         other,
-        pack,
-        neighbours,
+        *packs,
     )
     dense_away = swap_cores(dense_away)
-    here = call(here_kernel, out(slots, width + lane), core, act, hidden, down, pack, neighbours)
+    here = call(here_kernel, out(slots, width + lane), core, act, hidden, down, *packs)
     terms = call(join_kernel, out(ep_count, capacity, width + lane), here, expert_away, dense_away)
     returned = exchange(terms)
     return call(

time: 82.2 us -> 79.5 us (0.967)
  Pallas kernels: 10.3 us -> 5.84 us
  waiting for transfers between devices: 5.08 us -> 7.58 us
    pallas_call x9 -> x7, Pallas kernels: 10.3 us -> 5.84 us  [call(): pl.pallas_call(kernel, out_shape=outs, in_specs=specs, out_specs=[spec] *...]
    ppermute x3, waiting for transfers between devices: 4.2 us -> 6.9 us  [from_chip(): return lax.ppermute(value, EP, pairs)]
  transfers between devices with their start and end apart: 6 -> 6, of which waited for: 4 -> 4; matrix products, arithmetic and copies ran while one was open for 0% -> 0% of each run, Pallas kernels for 7% -> 4%
where the time goes in v1:
time: 79.5 us; the launch traced here: 79.3 us
  blocking collectives  62.6 us (79%)
  waiting for transfers between devices  7.58 us (10%)
  Pallas kernels  5.84 us (7%)
  starting transfers between devices  3.17 us (4%)
    all_to_all x2, blocking collectives, exchange(): return lax.all_to_all(rows, EP, split_axis=0, concat_axis=0, tiled=True)  62.6 us
    ppermute x3, waiting for transfers between devices, from_chip(): return lax.ppermute(value, EP, pairs)  6.9 us
    pallas_call x7, Pallas kernels, call(): pl.pallas_call(kernel, out_shape=outs, in_specs=specs, out_specs=[spec] *...  5.84 us
    ppermute x3, starting transfers between devices, from_chip(): return lax.ppermute(value, EP, pairs)  2.43 us
  transfers between devices with their start and end apart: 6, of which 4 were waited for; matrix products, arithmetic and copies ran while one was open for 0% of the time, Pallas kernels for 4%

profile of v1, /device:TPU:514, one launch (start us, length us, event | category | flops | bytes accessed | tf_op | source)
XLA Modules:
  0.0 79.3 jit_solution(3815369554678104240)
XLA Ops:
  0.0 0.0 copy-start
  0.0 1.4 %shard_map.109 = (bf16[64,2,1536]{2,1,0:T(2,128)(2,1)S(1)}, bf16[32,4736]{1,0:T(8,128)(2,1)S(1)}) custom-call(s32[1]{0:T(128)} %bitcast.core, bf16[8,1536]{1,0:T(8,128)(2,1)} %tokens_hbm.1, s32[4,8]{1,0:T(4,128)} %bitcast.7, f32[12,128]{1,0:T(8,128)} %bitcast.12, bf16[1,32]{1,0:T(2,128)(2,1)} %bitcast.13, bf16[32,1536]{1,0:T(8,128)(2,1)} %bitcast.10, ...), custom_call_target="tpu_custom_call" | custom-call | flops 1000000000 | tf_op jit(solution)/shard_map/pallas_call | solution.py:285
  1.4 37.4 %all_to_all.10.mine = bf16[64,2,1536]{2,1,0:T(2,128)(2,1)S(1)} all-to-all(bf16[64,2,1536]{2,1,0:T(2,128)(2,1)S(1)} %get-tuple-element.15), channel_id=1, replica_groups=mesh['grp'=2,'ep_0'=8,'ep_1'=8,'tp'=2] {'ep_0','ep_1'}, dimensions={0} | all-to-all | bytes 786432 | tf_op jit(solution)/shard_map/all_to_all | solution.py:319
  38.8 0.0 collective-permute-start
  38.8 0.9 %collective-permute-start.1 = (bf16[32,4736]{1,0:T(8,128)(2,1)S(1)}, bf16[32,4736]{1,0:T(8,128)(2,1)S(1)}, u32[]{:S(2)}, u32[]{:S(2)}) collective-permute-start(bf16[32,4736]{1,0:T(8,128)(2,1)S(1)} %get-tuple-element.20.refs_0_), channel_id=1, source_target_pairs={{2,0},{4,2},{6,4},{8,6},{10,8},{12,10},{14,12},{0,14},{18,16},{20,... | collective-permute-start | bytes 909320 | tf_op jit(solution)/shard_map/ppermute | solution.py:57
  39.7 1.2 %collective-permute-start.2 = (bf16[32,4736]{1,0:T(8,128)(2,1)S(1)}, bf16[32,4736]{1,0:T(8,128)(2,1)S(1)}, u32[]{:S(2)}, u32[]{:S(2)}) collective-permute-start(bf16[32,4736]{1,0:T(8,128)(2,1)S(1)} %get-tuple-element.20.refs_0_), channel_id=1, source_target_pairs={{14,0},{0,2},{2,4},{4,6},{6,8},{8,10},{10,12},{12,14},{30,16},{16,... | collective-permute-start | bytes 909320 | tf_op jit(solution)/shard_map/ppermute | solution.py:57
  40.9 0.4 collective-permute-start.3
  41.3 0.0 copy-done
  41.3 1.7 %shard_map.110 = (f32[128,768]{1,0:T(8,128)S(1)}, f32[128,768]{1,0:T(8,128)S(1)}, bf16[1536,768]{1,0:T(8,128)(2,1)S(1)}, f32[8,128]{1,0:T(8,128)S(1)}) custom-call(s32[1]{0:T(128)} %bitcast.core, bf16[64,2,1536]{2,1,0:T(2,128)(2,1)S(1)} %all_to_all.10.mine, bf16[1,1536,768]{2,1,0:T(8,128)(2,1)S(1)} %copy-done, bf16[1,1536,768]{2,1,0:T(8,128)(2,1)} %up_hbm.1, ...), custom_call_target="tpu_custom_call" | custom-call | flops 1000000000 | tf_op jit(solution)/shard_map/pallas_call | solution.py:285
  43.0 0.0 copy-start.1
  43.0 5.4 %collective-permute-done.1.refs_1_ = bf16[32,4736]{1,0:T(8,128)(2,1)S(1)} collective-permute-done((bf16[32,4736]{1,0:T(8,128)(2,1)S(1)}, bf16[32,4736]{1,0:T(8,128)(2,1)S(1)}, u32[]{:S(2)}, u32[]{:S(2)}) %collective-permute-start.1) | collective-permute-done | bytes 303136 | tf_op jit(solution)/shard_map/ppermute | solution.py:57
  48.4 0.6 collective-permute-done.2.refs_2_
  49.0 0.9 %collective-permute-done.3.refs_3_ = bf16[32,4736]{1,0:T(8,128)(2,1)S(1)} collective-permute-done((bf16[32,4736]{1,0:T(8,128)(2,1)S(1)}, bf16[32,4736]{1,0:T(8,128)(2,1)S(1)}, u32[]{:S(2)}, u32[]{:S(2)}) %collective-permute-start.3) | collective-permute-done | bytes 303136 | tf_op jit(solution)/shard_map/ppermute | solution.py:57
  49.9 0.0 collective-permute-done.other
  49.9 0.6 shard_map.112
  50.5 0.1 collective-permute-start.5
  50.6 0.0 copy-done.1
  50.6 0.8 shard_map.111
  51.4 0.6 collective-permute-start.4
  52.0 0.4 shard_map.113.here
  52.4 0.7 collective-permute-done.4.expert_away
  53.1 0.0 collective-permute-done.5.dense_away
  53.1 0.2 shard_map.114
  53.2 25.2 %all_to_all.11.returned = bf16[64,2,1664]{2,1,0:T(2,128)(2,1)S(1)} all-to-all(bf16[64,2,1664]{2,1,0:T(2,128)(2,1)S(1)} %shard_map.114), channel_id=1, replica_groups=mesh['grp'=2,'ep_0'=8,'ep_1'=8,'tp'=2] {'ep_0','ep_1'}, dimensions={0} | all-to-all | bytes 851968 | tf_op jit(solution)/shard_map/all_to_all | solution.py:319
  78.5 0.9 %shard_map.115 = bf16[8,768]{1,0:T(8,128)(2,1)} custom-call(bf16[64,2,1664]{2,1,0:T(2,128)(2,1)S(1)} %all_to_all.11.returned, f32[8,128]{1,0:T(8,128)S(1)} %get-tuple-element.24.combine), custom_call_target="tpu_custom_call" | custom-call | flops 1000000000 | tf_op jit(solution)/shard_map/pallas_call | solution.py:285
Async XLA Ops:
  0.0 41.3 %copy-start = (bf16[1,1536,768]{2,1,0:T(8,128)(2,1)S(1)}, bf16[1,1536,768]{2,1,0:T(8,128)(2,1)}, u32[]{:S(2)}) copy-start(bf16[1,1536,768]{2,1,0:T(8,128)(2,1)} %gate.3) | copy-start | bytes 7077892
  38.8 11.1 %collective-permute-start = (bf16[64,2,1536]{2,1,0:T(2,128)(2,1)S(1)}, bf16[64,2,1536]{2,1,0:T(2,128)(2,1)S(1)}, u32[]{:S(2)}, u32[]{:S(2)}) collective-permute-start(bf16[64,2,1536]{2,1,0:T(2,128)(2,1)S(1)} %all_to_all.10.mine), channel_id=1, source_target_pairs={{0,1},{1,0},{2,3},{3,2},{4,5},{5,4},{6,7},{7,6},{8,9},{9,8},{10,11... | collective-permute-start | bytes 1179656 | tf_op jit(solution)/shard_map/ppermute | solution.py:47
  38.8 9.6 %collective-permute-start.1 = (bf16[32,4736]{1,0:T(8,128)(2,1)S(1)}, bf16[32,4736]{1,0:T(8,128)(2,1)S(1)}, u32[]{:S(2)}, u32[]{:S(2)}) collective-permute-start(bf16[32,4736]{1,0:T(8,128)(2,1)S(1)} %get-tuple-element.20.refs_0_), channel_id=1, source_target_pairs={{2,0},{4,2},{6,4},{8,6},{10,8},{12,10},{14,12},{0,14},{18,16},{20,... | collective-permute-start | bytes 909320 | tf_op jit(solution)/shard_map/ppermute | solution.py:57
  39.7 9.3 %collective-permute-start.2 = (bf16[32,4736]{1,0:T(8,128)(2,1)S(1)}, bf16[32,4736]{1,0:T(8,128)(2,1)S(1)}, u32[]{:S(2)}, u32[]{:S(2)}) collective-permute-start(bf16[32,4736]{1,0:T(8,128)(2,1)S(1)} %get-tuple-element.20.refs_0_), channel_id=1, source_target_pairs={{14,0},{0,2},{2,4},{4,6},{6,8},{8,10},{10,12},{12,14},{30,16},{16,... | collective-permute-start | bytes 909320 | tf_op jit(solution)/shard_map/ppermute | solution.py:57
  40.9 9.0 %collective-permute-start.3 = (bf16[32,4736]{1,0:T(8,128)(2,1)S(1)}, bf16[32,4736]{1,0:T(8,128)(2,1)S(1)}, u32[]{:S(2)}, u32[]{:S(2)}) collective-permute-start(bf16[32,4736]{1,0:T(8,128)(2,1)S(1)} %get-tuple-element.20.refs_0_), channel_id=1, source_target_pairs={{16,0},{18,2},{20,4},{22,6},{24,8},{26,10},{28,12},{30,14},{32,16}... | collective-permute-start | bytes 909320 | tf_op jit(solution)/shard_map/ppermute | solution.py:57
  43.0 7.6 %copy-start.1 = (bf16[1,768,1536]{2,1,0:T(8,128)(2,1)S(1)}, bf16[1,768,1536]{2,1,0:T(8,128)(2,1)}, u32[]{:S(2)}) copy-start(bf16[1,768,1536]{2,1,0:T(8,128)(2,1)} %down.3) | copy-start | bytes 7077892
  50.5 2.6 %collective-permute-start.5 = (bf16[128,896]{1,0:T(8,128)(2,1)S(1)}, bf16[128,896]{1,0:T(8,128)(2,1)S(1)}, u32[]{:S(2)}, u32[]{:S(2)}) collective-permute-start(bf16[128,896]{1,0:T(8,128)(2,1)S(1)} %get-tuple-element.23), channel_id=1, source_target_pairs={{0,1},{1,0},{2,3},{3,2},{4,5},{5,4},{6,7},{7,6},{8,9},{9,8},{10,11... | collective-permute-start | bytes 688136 | tf_op jit(solution)/shard_map/ppermute | solution.py:47
  51.4 1.7 %collective-permute-start.4 = (bf16[128,768]{1,0:T(8,128)(2,1)S(1)}, bf16[128,768]{1,0:T(8,128)(2,1)S(1)}, u32[]{:S(2)}, u32[]{:S(2)}) collective-permute-start(bf16[128,768]{1,0:T(8,128)(2,1)S(1)} %get-tuple-element.22), channel_id=1, source_target_pairs={{0,1},{1,0},{2,3},{3,2},{4,5},{5,4},{6,7},{7,6},{8,9},{9,8},{10,11... | collective-permute-start | bytes 589832 | tf_op jit(solution)/shard_map/ppermute | solution.py:47

commit v2 on v1

--- a/solution.py
+++ b/solution.py
@@ -19,8 +19,7 @@
 norm_eps = 1e-06
 capacity = 2
 lane = 128
-shape = ((0, 0), (0, 1), (0, -1), (1, 0))
-classes = len(shape)
+classes = 4
 
 F32, BF16, I32 = jnp.float32, jnp.bfloat16, jnp.int32
 
@@ -47,14 +46,21 @@
     return lax.ppermute(value, "tp", [(0, 1), (1, 0)])
 
 
-def from_chip(value, down, across):
+def from_partner(value, partner):
     high, wide = lax.axis_size("ep_0"), lax.axis_size("ep_1")
-    pairs = [
-        ((y + down) % high * wide + (x + across) % wide, y * wide + x)
-        for y in range(high)
-        for x in range(wide)
-    ]
+    pairs = []
+    for y in range(high):
+        for x in range(wide):
+            row, column = partner(y, x)
+            pairs.append((y * wide + x, row % high * wide + column % wide))
     return lax.ppermute(value, EP, pairs)
+
+
+partners = (
+    lambda y, x: (y, x ^ 1),
+    lambda y, x: (y, ((x + 1) ^ 1) - 1),
+    lambda y, x: (y ^ 1, x),
+)
 
 
 def class_of(chip, wide):
@@ -162,22 +168,15 @@
     return at, to
 
 
-def own_kernel(
-    core,
-    mine,
-    gate,
-    up_hbm,
-    routes_hbm,
-    weights_hbm,
-    gate_pre,
-    up_pre,
-    up,
-    combine,
-    routes,
-    weights,
-    sems,
-):
+def rows(packs, start, size):
+    return jnp.concatenate([p[:, pl.ds(start, size)] for p in packs], axis=0)
+
+
+def own_kernel(core, mine, gate, up_hbm, down_hbm, routes_hbm, weights_hbm, *refs):
+    packs = refs[:classes]
+    gate_pre, up_pre, dense_gate, dense_up, up, down, combine, routes, weights, sems = refs[classes:]
     half = mine.shape[2] // 2
+    width = 2 * half
     at, to = halves(core, half)
     copies = copy_all(
         (
@@ -185,17 +184,22 @@
             (routes_hbm, routes),
             (weights_hbm, weights),
             (up_hbm.at[0, pl.ds(to, half), :], up.at[pl.ds(to, half), :]),
+            (down_hbm.at[0, :, pl.ds(to, half)], down),
         ),
         sems,
     )
     x = mine[:, :, :half].reshape(-1, half)
     gate_pre[...] = dot(x, gate[0, pl.ds(at, half), :])
+    z = mine[:, :, half:].reshape(-1, half)
+    dense_gate[...] = dot_nt(z, rows(packs, at, half))
+    dense_up[...] = dot_nt(z, rows(packs, width + at, half))
     copies[1].wait()
     copies[2].wait()
     weigh(routes, weights, combine)
     copies[0].wait()
     up_pre[...] = dot(x, up[pl.ds(at, half), :])
-    copies[3].wait()
+    for copy in copies[3:]:
+        copy.wait()
 
 
 def rest_kernel(core, other, gate_pre, up_pre, gate, up, down, act, away):
@@ -207,37 +211,35 @@
         up_pre[...] + dot(y, up[pl.ds(to, half), :]),
     )
     act[...] = value
-    away[...] = dot(value, down[0, :, pl.ds(to, half)]).astype(BF16)
-
-
-def rows(packs, start, size):
-    return jnp.concatenate([p[:, pl.ds(start, size)] for p in packs], axis=0)
-
-
-def dense_kernel(core, mine, other, *refs):
+    away[...] = dot(value, down[...]).astype(BF16)
+
+
+def dense_kernel(core, other, dense_gate, dense_up, *refs):
     packs, (hidden, away) = refs[:classes], refs[classes:]
-    half = mine.shape[2] // 2
+    half = other.shape[2] // 2
     width = 2 * half
-    at, to = halves(core, half)
-    x = mine[:, :, half:].reshape(-1, half)
-    y = other[:, :, half:].reshape(-1, half)
-    gate_pre = dot_nt(x, rows(packs, at, half)) + dot_nt(y, rows(packs, to, half))
-    up_pre = dot_nt(x, rows(packs, width + at, half)) + dot_nt(y, rows(packs, width + to, half))
-    value = clamped_unit(gate_pre, up_pre)
+    _, to = halves(core, half)
+    z = other[:, :, half:].reshape(-1, half)
+    value = clamped_unit(
+        dense_gate[...] + dot_nt(z, rows(packs, to, half)),
+        dense_up[...] + dot_nt(z, rows(packs, width + to, half)),
+    )
     hidden[...] = value
     away[:, :half] = dot(value, rows(packs, 2 * width + to, half)).astype(BF16)
     away[:, half:] = dot(value, rows(packs, 3 * width, lane)).astype(BF16)
 
 
-def here_kernel(core, act, hidden, down, *refs):
-    packs, out = refs[:classes], refs[classes]
-    half = down.shape[2] // 2
+def here_kernel(core, act, hidden, down_hbm, *refs):
+    packs, (out, down, sems) = refs[:classes], refs[classes:]
+    half = down.shape[1]
     width = 2 * half
     at, _ = halves(core, half)
-    out[:, :half] = dot(act[...], down[0, :, pl.ds(at, half)]).astype(BF16)
+    (copy,) = copy_all(((down_hbm.at[0, :, pl.ds(at, half)], down),), sems)
     value = hidden[...]
     out[:, half:width] = dot(value, rows(packs, 2 * width + at, half)).astype(BF16)
     out[:, width:] = dot(value, rows(packs, 3 * width, lane)).astype(BF16)
+    copy.wait()
+    out[:, :half] = dot(act[...], down[...]).astype(BF16)
 
 
 def join_kernel(here, expert_away, dense_away, out):
@@ -268,10 +270,10 @@
     out[...] = (jax.nn.sigmoid(gate_logit) * dense_out + expert_mix).astype(BF16)
 
 
-def call(kernel, outs, *operands, inside=0, scratch=(), room=8 * 2**20):
+def call(kernel, outs, *operands, inside=(), scratch=(), room=8 * 2**20):
     specs, placed = [], []
     for n, operand in enumerate(operands):
-        if n >= len(operands) - inside:
+        if n in inside:
             specs.append(pl.BlockSpec(memory_space=pl.ANY))
             placed.append(pltpu.with_memory_space_constraint(operand, pltpu.HBM))
         elif operand.dtype == I32 and operand.ndim == 1:
@@ -333,7 +335,7 @@
         dense_gate.T,
         dense_up.T,
         dense_down,
-        inside=7,
+        inside=range(1, 8),
         scratch=(
             pltpu.VMEM((tok_dev, width), BF16),
             pltpu.VMEM((top, tok_dev), I32),
@@ -343,30 +345,47 @@
         ),
     )
     packs = [pack]
-    for offset in shape[1:]:
-        packs.append(from_chip(pack, *offset))
+    for partner in partners:
+        packs.append(from_partner(pack, partner))
     mine = exchange(outgoing)
-    gate, down = (
-        pltpu.with_memory_space_constraint(w, pltpu.VMEM) for w in (expert_gate, expert_down)
-    )
+    gate = pltpu.with_memory_space_constraint(expert_gate, pltpu.VMEM)
     other = swap_cores(mine)
-    gate_pre, up_pre, up, combine = call(
+    sums = [out(slots, hidden_units, dtype=F32)] * 2
+    dense_sums = [out(slots, classes * units, dtype=F32)] * 2
+    gate_pre, up_pre, dense_gate_pre, dense_up_pre, up, down, combine = call(
         own_kernel,
-        [out(slots, hidden_units, dtype=F32)] * 2
-        + [out(width, hidden_units), out(tok_dev, slots, dtype=F32)],
+        sums
+        + dense_sums
+        + [
+            out(width, hidden_units),
+            out(hidden_units, half),
+            out(tok_dev, slots, dtype=F32),
+        ],
         core,
         mine,
         gate,
         expert_up,
+        expert_down,
         routes.T,
         route_weight.T,
-        inside=3,
+        *packs,
+        inside=(3, 4, 5, 6),
         scratch=(
             pltpu.VMEM((top, tok_dev), I32),
             pltpu.VMEM((top, tok_dev), F32),
-            dma((4,)),
+            dma((5,)),
         ),
     )
+    hidden, dense_away = call(
+        dense_kernel,
+        [out(slots, classes * units), out(slots, half + lane)],
+        core,
+        other,
+        dense_gate_pre,
+        dense_up_pre,
+        *packs,
+    )
+    dense_away = swap_cores(dense_away)
     act, expert_away = call(
         rest_kernel,
         [out(slots, hidden_units), out(slots, half)],
@@ -379,16 +398,17 @@
         down,
     )
     expert_away = swap_cores(expert_away)
-    hidden, dense_away = call(
-        dense_kernel,
-        [out(slots, classes * units), out(slots, half + lane)],
+    here = call(
+        here_kernel,
+        out(slots, width + lane),
         core,
-        mine,
-        other,
+        act,
+        hidden,
+        expert_down,
         *packs,
-    )
-    dense_away = swap_cores(dense_away)
-    here = call(here_kernel, out(slots, width + lane), core, act, hidden, down, *packs)
+        inside=(3,),
+        scratch=(pltpu.VMEM((hidden_units, half), BF16), dma((1,))),
+    )
     terms = call(join_kernel, out(ep_count, capacity, width + lane), here, expert_away, dense_away)
     returned = exchange(terms)
     return call(

time: 79.5 us -> 79.2 us (level)
  blocking collectives: 62.6 us -> 26.4 us
  starting transfers between devices: 3.17 us -> 30.1 us
  Pallas kernels: 5.84 us -> 11.7 us
  waiting for transfers between devices: 7.58 us -> 10.1 us
    all_to_all x2 -> x1, blocking collectives: 62.6 us -> 26.4 us  [exchange(): return lax.all_to_all(rows, EP, split_axis=0, concat_axis=0, tiled=True)]
    all_to_all x0 -> x1, starting transfers between devices: none -> 24.2 us  [exchange(): return lax.all_to_all(rows, EP, split_axis=0, concat_axis=0, tiled=True)]
    all_to_all x0 -> x1, waiting for transfers between devices: none -> 10.1 us  [exchange(): return lax.all_to_all(rows, EP, split_axis=0, concat_axis=0, tiled=True)]
    ppermute x3, waiting for transfers between devices: 6.9 us -> 0.01 us  [from_partner(): return lax.ppermute(value, EP, pairs)]
    pallas_call x7, Pallas kernels: 5.84 us -> 11.7 us  [call(): pl.pallas_call(kernel, out_shape=outs, in_specs=specs, out_specs=[spec] *...]
    ppermute x3, starting transfers between devices: 2.43 us -> 5.1 us  [from_partner(): return lax.ppermute(value, EP, pairs)]
  transfers between devices with their start and end apart: 6 -> 7, of which waited for: 4 -> 1; matrix products, arithmetic and copies ran while one was open for 0% -> 0% of each run, Pallas kernels for 4% -> 9%
where the time goes in v2:
time: 79.2 us; the launch traced here: 78.4 us
  starting transfers between devices  30.1 us (38%)
  blocking collectives  26.4 us (33%)
  Pallas kernels  11.7 us (15%)
  waiting for transfers between devices  10.1 us (13%)
    all_to_all x1, blocking collectives, exchange(): return lax.all_to_all(rows, EP, split_axis=0, concat_axis=0, tiled=True)  26.4 us
    all_to_all x1, starting transfers between devices, exchange(): return lax.all_to_all(rows, EP, split_axis=0, concat_axis=0, tiled=True)  24.2 us
    pallas_call x7, Pallas kernels, call(): pl.pallas_call(kernel, out_shape=outs, in_specs=specs, out_specs=[spec] *...  11.7 us
    all_to_all x1, waiting for transfers between devices, exchange(): return lax.all_to_all(rows, EP, split_axis=0, concat_axis=0, tiled=True)  10.1 us
    ppermute x3, starting transfers between devices, from_partner(): return lax.ppermute(value, EP, pairs)  5.1 us
  transfers between devices with their start and end apart: 7, of which 1 were waited for; matrix products, arithmetic and copies ran while one was open for 0% of the time, Pallas kernels for 9%

profile of v2, /device:TPU:514, one launch (start us, length us, event | category | flops | bytes accessed | tf_op | source)
XLA Modules:
  0.0 78.4 jit_solution(11861421462136356065)
XLA Ops:
  0.0 0.0 copy-start
  0.0 2.1 %shard_map.109 = (bf16[64,2,1536]{2,1,0:T(2,128)(2,1)}, bf16[32,4736]{1,0:T(8,128)(2,1)S(1)}) custom-call(s32[1]{0:T(128)} %bitcast.core, bf16[8,1536]{1,0:T(8,128)(2,1)} %tokens_hbm.1, s32[4,8]{1,0:T(4,128)} %bitcast.7, f32[12,128]{1,0:T(8,128)} %bitcast.12, bf16[1,32]{1,0:T(2,128)(2,1)} %bitcast.13, bf16[32,1536]{1,0:T(8,128)(2,1)} %bitcast.10, ...), custom_call_target="tpu_custom_call" | custom-call | flops 1000000000 | tf_op jit(solution)/shard_map/pallas_call | solution.py:287
  2.1 24.2 %all-to-all-start = ((bf16[64,2,1536]{2,1,0:T(2,128)(2,1)}), bf16[64,2,1536]{2,1,0:T(2,128)(2,1)S(1)}, u32[]{:S(2)}, u32[]{:S(2)}) async-start(bf16[64,2,1536]{2,1,0:T(2,128)(2,1)} %get-tuple-element.18), calls=%async_computation | async-start | bytes 786432 | tf_op jit(solution)/shard_map/all_to_all | solution.py:321
  26.4 1.7 %collective-permute-start.3 = (bf16[32,4736]{1,0:T(8,128)(2,1)S(1)}, bf16[32,4736]{1,0:T(8,128)(2,1)S(1)}, u32[]{:S(2)}, u32[]{:S(2)}) collective-permute-start(bf16[32,4736]{1,0:T(8,128)(2,1)S(1)} %get-tuple-element.19.refs_0_), channel_id=1, source_target_pairs={{0,16},{2,18},{4,20},{6,22},{8,24},{10,26},{12,28},{14,30},{16,0},... | collective-permute-start | bytes 909320 | tf_op jit(solution)/shard_map/ppermute | solution.py:56
  28.1 1.5 %collective-permute-start.2 = (bf16[32,4736]{1,0:T(8,128)(2,1)S(1)}, bf16[32,4736]{1,0:T(8,128)(2,1)}, u32[]{:S(2)}, u32[]{:S(2)}) collective-permute-start(bf16[32,4736]{1,0:T(8,128)(2,1)S(1)} %get-tuple-element.19.refs_0_), channel_id=1, source_target_pairs={{0,14},{2,4},{4,2},{6,8},{8,6},{10,12},{12,10},{14,0},{16,30},{18,... | collective-permute-start | bytes 909320 | tf_op jit(solution)/shard_map/ppermute | solution.py:56
  29.6 1.9 %collective-permute-start.1 = (bf16[32,4736]{1,0:T(8,128)(2,1)S(1)}, bf16[32,4736]{1,0:T(8,128)(2,1)}, u32[]{:S(2)}, u32[]{:S(2)}) collective-permute-start(bf16[32,4736]{1,0:T(8,128)(2,1)S(1)} %get-tuple-element.19.refs_0_), channel_id=1, source_target_pairs={{0,2},{2,0},{4,6},{6,4},{8,10},{10,8},{12,14},{14,12},{16,18},{18,... | collective-permute-start | bytes 909320 | tf_op jit(solution)/shard_map/ppermute | solution.py:56
  31.5 10.1 %all-to-all-done.mine = bf16[64,2,1536]{2,1,0:T(2,128)(2,1)S(1)} async-done(((bf16[64,2,1536]{2,1,0:T(2,128)(2,1)}), bf16[64,2,1536]{2,1,0:T(2,128)(2,1)S(1)}, u32[]{:S(2)}, u32[]{:S(2)}) %all-to-all-start) | async-done | bytes 393248 | tf_op jit(solution)/shard_map/all_to_all | solution.py:321
  41.6 0.0 collective-permute-start
  41.6 0.0 collective-permute-done.3.refs_3_
  41.6 0.0 collective-permute-done.2.refs_2_
  41.6 0.0 collective-permute-done.1.refs_1_
  41.6 0.0 copy-done
  41.6 3.5 %shard_map.110 = (f32[128,768]{1,0:T(8,128)S(1)}, f32[128,768]{1,0:T(8,128)S(1)}, f32[128,128]{1,0:T(8,128)S(1)}, f32[128,128]{1,0:T(8,128)S(1)}, bf16[1536,768]...) custom-call(s32[1]{0:T(128)} %bitcast.core, bf16[64,2,1536]{2,1,0:T(2,128)(2,1)S(1)} %all-to-all-done.mine, ...), custom_call_target="tpu_custom_call" | custom-call | flops 1000000000 | tf_op jit(solution)/shard_map/pallas_call | solution.py:287
  45.2 0.0 collective-permute-done.other
  45.2 1.5 %shard_map.112 = (bf16[128,128]{1,0:T(8,128)(2,1)S(1)}, bf16[128,896]{1,0:T(8,128)(2,1)S(1)}) custom-call(s32[1]{0:T(128)} %bitcast.core, bf16[64,2,1536]{2,1,0:T(2,128)(2,1)S(1)} %collective-permute-done.other, f32[128,128]{1,0:T(8,128)S(1)} %get-tuple-element.25.dense_gate, f32[128,128]{1,0:T(8,128)S(1)} %get-tuple-element.26.dense_up, ...), custom_call_target="tpu_custom_call" | custom-call | flops 1000000000 | tf_op jit(solution)/shard_map/pallas_call | solution.py:287
  46.7 0.6 collective-permute-start.5
  47.3 0.8 shard_map.111
  48.1 0.2 collective-permute-start.4
  48.2 2.7 %shard_map.113.here = bf16[128,1664]{1,0:T(8,128)(2,1)S(1)} custom-call(s32[1]{0:T(128)} %bitcast.core, bf16[128,768]{1,0:T(8,128)(2,1)S(1)} %get-tuple-element.24.act, bf16[128,128]{1,0:T(8,128)(2,1)S(1)} %get-tuple-element.27.hidden, bf16[1,768,1536]{2,1,0:T(8,128)(2,1)} %down_hbm.5, bf16[32,4736]{1,0:T(8,128)(2,1)S(1)} %get-tuple-element.19.refs_0_, ...), custom_call_target="tpu_custom_call" | custom-call | flops 1000000000 | tf_op jit(solution)/shard_map/pallas_call | solution.py:287
  51.0 0.0 collective-permute-done.4.expert_away
  51.0 0.0 collective-permute-done.5.dense_away
  51.0 0.2 shard_map.114
  51.2 26.4 %all_to_all.10.returned = bf16[64,2,1664]{2,1,0:T(2,128)(2,1)S(1)} all-to-all(bf16[64,2,1664]{2,1,0:T(2,128)(2,1)S(1)} %shard_map.114), channel_id=1, replica_groups=mesh['grp'=2,'ep_0'=8,'ep_1'=8,'tp'=2] {'ep_0','ep_1'}, dimensions={0} | all-to-all | bytes 851968 | tf_op jit(solution)/shard_map/all_to_all | solution.py:321
  77.6 0.9 %shard_map.115 = bf16[8,768]{1,0:T(8,128)(2,1)} custom-call(bf16[64,2,1664]{2,1,0:T(2,128)(2,1)S(1)} %all_to_all.10.returned, f32[8,128]{1,0:T(8,128)S(1)} %get-tuple-element.30.combine), custom_call_target="tpu_custom_call" | custom-call | flops 1000000000 | tf_op jit(solution)/shard_map/pallas_call | solution.py:287
Async XLA Ops:
  0.0 41.6 %copy-start = (bf16[1,1536,768]{2,1,0:T(8,128)(2,1)S(1)}, bf16[1,1536,768]{2,1,0:T(8,128)(2,1)}, u32[]{:S(2)}) copy-start(bf16[1,1536,768]{2,1,0:T(8,128)(2,1)} %gate.3) | copy-start | bytes 7077892
  2.1 39.5 %all-to-all-start = ((bf16[64,2,1536]{2,1,0:T(2,128)(2,1)}), bf16[64,2,1536]{2,1,0:T(2,128)(2,1)S(1)}, u32[]{:S(2)}, u32[]{:S(2)}) async-start(bf16[64,2,1536]{2,1,0:T(2,128)(2,1)} %get-tuple-element.18), calls=%async_computation | async-start | bytes 786432 | tf_op jit(solution)/shard_map/all_to_all | solution.py:321
  26.4 15.2 %collective-permute-start.3 = (bf16[32,4736]{1,0:T(8,128)(2,1)S(1)}, bf16[32,4736]{1,0:T(8,128)(2,1)S(1)}, u32[]{:S(2)}, u32[]{:S(2)}) collective-permute-start(bf16[32,4736]{1,0:T(8,128)(2,1)S(1)} %get-tuple-element.19.refs_0_), channel_id=1, source_target_pairs={{0,16},{2,18},{4,20},{6,22},{8,24},{10,26},{12,28},{14,30},{16,0},... | collective-permute-start | bytes 909320 | tf_op jit(solution)/shard_map/ppermute | solution.py:56
  28.1 13.5 %collective-permute-start.2 = (bf16[32,4736]{1,0:T(8,128)(2,1)S(1)}, bf16[32,4736]{1,0:T(8,128)(2,1)}, u32[]{:S(2)}, u32[]{:S(2)}) collective-permute-start(bf16[32,4736]{1,0:T(8,128)(2,1)S(1)} %get-tuple-element.19.refs_0_), channel_id=1, source_target_pairs={{0,14},{2,4},{4,2},{6,8},{8,6},{10,12},{12,10},{14,0},{16,30},{18,... | collective-permute-start | bytes 909320 | tf_op jit(solution)/shard_map/ppermute | solution.py:56
  29.6 12.0 %collective-permute-start.1 = (bf16[32,4736]{1,0:T(8,128)(2,1)S(1)}, bf16[32,4736]{1,0:T(8,128)(2,1)}, u32[]{:S(2)}, u32[]{:S(2)}) collective-permute-start(bf16[32,4736]{1,0:T(8,128)(2,1)S(1)} %get-tuple-element.19.refs_0_), channel_id=1, source_target_pairs={{0,2},{2,0},{4,6},{6,4},{8,10},{10,8},{12,14},{14,12},{16,18},{18,... | collective-permute-start | bytes 909320 | tf_op jit(solution)/shard_map/ppermute | solution.py:56
  41.6 3.6 %collective-permute-start = (bf16[64,2,1536]{2,1,0:T(2,128)(2,1)S(1)}, bf16[64,2,1536]{2,1,0:T(2,128)(2,1)S(1)}, u32[]{:S(2)}, u32[]{:S(2)}) collective-permute-start(bf16[64,2,1536]{2,1,0:T(2,128)(2,1)S(1)} %all-to-all-done.mine), channel_id=1, source_target_pairs={{0,1},{1,0},{2,3},{3,2},{4,5},{5,4},{6,7},{7,6},{8,9},{9,8},{10,11... | collective-permute-start | bytes 1179656 | tf_op jit(solution)/shard_map/ppermute | solution.py:46
  46.7 4.3 %collective-permute-start.5 = (bf16[128,896]{1,0:T(8,128)(2,1)S(1)}, bf16[128,896]{1,0:T(8,128)(2,1)S(1)}, u32[]{:S(2)}, u32[]{:S(2)}) collective-permute-start(bf16[128,896]{1,0:T(8,128)(2,1)S(1)} %get-tuple-element.29), channel_id=1, source_target_pairs={{0,1},{1,0},{2,3},{3,2},{4,5},{5,4},{6,7},{7,6},{8,9},{9,8},{10,11... | collective-permute-start | bytes 688136 | tf_op jit(solution)/shard_map/ppermute | solution.py:46
  48.1 2.9 %collective-permute-start.4 = (bf16[128,768]{1,0:T(8,128)(2,1)S(1)}, bf16[128,768]{1,0:T(8,128)(2,1)S(1)}, u32[]{:S(2)}, u32[]{:S(2)}) collective-permute-start(bf16[128,768]{1,0:T(8,128)(2,1)S(1)} %get-tuple-element.28), channel_id=1, source_target_pairs={{0,1},{1,0},{2,3},{3,2},{4,5},{5,4},{6,7},{7,6},{8,9},{9,8},{10,11... | collective-permute-start | bytes 589832 | tf_op jit(solution)/shard_map/ppermute | solution.py:46

commit v3 on v2

--- a/solution.py
+++ b/solution.py
@@ -63,6 +63,10 @@
 )
 
 
+def expert_of(rank, high, wide):
+    return rank % high * wide + rank // high
+
+
 def class_of(chip, wide):
     return (chip % wide + 2 * (chip // wide)) % classes
 
@@ -75,6 +79,7 @@
 
 
 def first_kernel(
+    high,
     wide,
     core,
     tokens_hbm,
@@ -112,7 +117,7 @@
     units = pack.shape[0]
     slot = iota((slots, tok_dev), 0)
     row = iota((slots, tok_dev), 1)
-    expert = slot // capacity
+    expert = expert_of(slot // capacity, high, wide)
     share = tok_dev // classes
     wanted = (row == class_of(expert, wide) * share + slot % capacity).astype(F32).astype(BF16)
     earlier = (iota((tok_dev, tok_dev), 0) < iota((tok_dev, tok_dev), 1)).astype(F32).astype(BF16)
@@ -144,10 +149,11 @@
         copy.wait()
 
 
-def weigh(routes, weights, combine):
+def weigh(high, wide, routes, weights, combine):
     top, tok_dev = routes.shape
     slots = combine.shape[1]
     slot = iota((tok_dev, slots), 1)
+    expert = expert_of(slot // capacity, high, wide)
     eye = iota((tok_dev, tok_dev), 0) == iota((tok_dev, tok_dev), 1)
     earlier = (iota((tok_dev, tok_dev), 1) < iota((tok_dev, tok_dev), 0)).astype(F32).astype(BF16)
     member = jnp.zeros((tok_dev, slots), F32)
@@ -155,7 +161,7 @@
     for k in range(top):
         named = jnp.sum(jnp.where(eye, routes[k : k + 1, :], 0), axis=1, keepdims=True)
         worth = jnp.sum(jnp.where(eye, weights[k : k + 1, :], 0.0), axis=1, keepdims=True)
-        hit = named == slot // capacity
+        hit = named == expert
         member = jnp.where(hit, 1.0, member)
         weight = jnp.where(hit, worth, weight)
     rank = dot(earlier, member.astype(BF16))
@@ -172,34 +178,22 @@
     return jnp.concatenate([p[:, pl.ds(start, size)] for p in packs], axis=0)
 
 
-def own_kernel(core, mine, gate, up_hbm, down_hbm, routes_hbm, weights_hbm, *refs):
+def own_kernel(high, wide, core, mine, gate, up, routes_hbm, weights_hbm, *refs):
     packs = refs[:classes]
-    gate_pre, up_pre, dense_gate, dense_up, up, down, combine, routes, weights, sems = refs[classes:]
+    gate_pre, up_pre, dense_gate, dense_up, combine, routes, weights, sems = refs[classes:]
     half = mine.shape[2] // 2
     width = 2 * half
-    at, to = halves(core, half)
-    copies = copy_all(
-        (
-            (up_hbm.at[0, pl.ds(at, half), :], up.at[pl.ds(at, half), :]),
-            (routes_hbm, routes),
-            (weights_hbm, weights),
-            (up_hbm.at[0, pl.ds(to, half), :], up.at[pl.ds(to, half), :]),
-            (down_hbm.at[0, :, pl.ds(to, half)], down),
-        ),
-        sems,
-    )
+    at, _ = halves(core, half)
+    copies = copy_all(((routes_hbm, routes), (weights_hbm, weights)), sems)
     x = mine[:, :, :half].reshape(-1, half)
     gate_pre[...] = dot(x, gate[0, pl.ds(at, half), :])
+    up_pre[...] = dot(x, up[0, pl.ds(at, half), :])
     z = mine[:, :, half:].reshape(-1, half)
     dense_gate[...] = dot_nt(z, rows(packs, at, half))
     dense_up[...] = dot_nt(z, rows(packs, width + at, half))
-    copies[1].wait()
-    copies[2].wait()
-    weigh(routes, weights, combine)
-    copies[0].wait()
-    up_pre[...] = dot(x, up[pl.ds(at, half), :])
-    for copy in copies[3:]:
+    for copy in copies:
         copy.wait()
+    weigh(high, wide, routes, weights, combine)
 
 
 def rest_kernel(core, other, gate_pre, up_pre, gate, up, down, act, away):
@@ -208,10 +202,10 @@
     y = other[:, :, :half].reshape(-1, half)
     value = clamped_unit(
         gate_pre[...] + dot(y, gate[0, pl.ds(to, half), :]),
-        up_pre[...] + dot(y, up[pl.ds(to, half), :]),
+        up_pre[...] + dot(y, up[0, pl.ds(to, half), :]),
     )
     act[...] = value
-    away[...] = dot(value, down[...]).astype(BF16)
+    away[...] = dot(value, down[0, :, pl.ds(to, half)]).astype(BF16)
 
 
 def dense_kernel(core, other, dense_gate, dense_up, *refs):
@@ -229,17 +223,15 @@
     away[:, half:] = dot(value, rows(packs, 3 * width, lane)).astype(BF16)
 
 
-def here_kernel(core, act, hidden, down_hbm, *refs):
-    packs, (out, down, sems) = refs[:classes], refs[classes:]
-    half = down.shape[1]
+def here_kernel(core, act, hidden, down, *refs):
+    packs, out = refs[:classes], refs[classes]
+    half = down.shape[2] // 2
     width = 2 * half
     at, _ = halves(core, half)
-    (copy,) = copy_all(((down_hbm.at[0, :, pl.ds(at, half)], down),), sems)
+    out[:, :half] = dot(act[...], down[0, :, pl.ds(at, half)]).astype(BF16)
     value = hidden[...]
     out[:, half:width] = dot(value, rows(packs, 2 * width + at, half)).astype(BF16)
     out[:, width:] = dot(value, rows(packs, 3 * width, lane)).astype(BF16)
-    copy.wait()
-    out[:, :half] = dot(act[...], down[...]).astype(BF16)
 
 
 def join_kernel(here, expert_away, dense_away, out):
@@ -252,12 +244,13 @@
     out[:, :, half:] = dense.reshape(shape3)
 
 
-def mix_kernel(wide, returned, combine, out):
+def mix_kernel(high, wide, returned, combine, out):
     tok_dev, half = out.shape
     slots = returned.shape[0] * returned.shape[1]
     slot = iota((tok_dev, slots), 1)
     share = tok_dev // classes
-    owner = class_of(slot // capacity, wide) * share + slot % capacity
+    chip = expert_of(slot // capacity, high, wide)
+    owner = class_of(chip, wide) * share + slot % capacity
     wanted = (iota((tok_dev, slots), 0) == owner).astype(F32).astype(BF16)
     dense_out = dot(wanted, returned[:, :, half : 2 * half].reshape(slots, half))
     gate_logit = dot(wanted, returned[:, :, 2 * half :].reshape(slots, lane))[:, :1]
@@ -270,7 +263,7 @@
     out[...] = (jax.nn.sigmoid(gate_logit) * dense_out + expert_mix).astype(BF16)
 
 
-def call(kernel, outs, *operands, inside=(), scratch=(), room=8 * 2**20):
+def call(kernel, outs, *operands, inside=(), scratch=(), room=8 * 2**20, flops=10**6):
     specs, placed = [], []
     for n, operand in enumerate(operands):
         if n in inside:
@@ -290,7 +283,7 @@
         in_specs=specs,
         out_specs=[spec] * len(outs) if many else spec,
         scratch_shapes=list(scratch),
-        cost_estimate=pl.CostEstimate(flops=10**9, transcendentals=0, bytes_accessed=0),
+        cost_estimate=pl.CostEstimate(flops=flops, transcendentals=0, bytes_accessed=0),
         compiler_params=pltpu.CompilerParams(vmem_limit_bytes=room),
     )(*placed)
 
@@ -312,20 +305,20 @@
     top = routes.shape[1]
     half = width // lax.axis_size("tp")
     ep_count = lax.axis_size(EP)
-    wide = lax.axis_size("ep_1")
+    high, wide = lax.axis_size("ep_0"), lax.axis_size("ep_1")
     slots = ep_count * capacity
     units, hidden_units = dense_down.shape[0], expert_down.shape[1]
     core = lax.axis_index("tp").reshape(1)
 
     def exchange(rows):
-        return lax.all_to_all(rows, EP, split_axis=0, concat_axis=0, tiled=True)
+        return lax.all_to_all(rows, EP[::-1], split_axis=0, concat_axis=0, tiled=True)
 
     def out(*dims, dtype=BF16):
         return pltpu.VMEM(dims, dtype)
 
     dma = pltpu.SemaphoreType.DMA
     outgoing, pack = call(
-        functools.partial(first_kernel, wide),
+        functools.partial(first_kernel, high, wide),
         [out(ep_count, capacity, width), out(units, 3 * width + lane)],
         core,
         tokens,
@@ -336,6 +329,7 @@
         dense_up.T,
         dense_down,
         inside=range(1, 8),
+        flops=10**11,
         scratch=(
             pltpu.VMEM((tok_dev, width), BF16),
             pltpu.VMEM((top, tok_dev), I32),
@@ -348,32 +342,28 @@
     for partner in partners:
         packs.append(from_partner(pack, partner))
     mine = exchange(outgoing)
-    gate = pltpu.with_memory_space_constraint(expert_gate, pltpu.VMEM)
+    gate, up, down = (
+        pltpu.with_memory_space_constraint(w, pltpu.VMEM)
+        for w in (expert_gate, expert_up, expert_down)
+    )
     other = swap_cores(mine)
     sums = [out(slots, hidden_units, dtype=F32)] * 2
     dense_sums = [out(slots, classes * units, dtype=F32)] * 2
-    gate_pre, up_pre, dense_gate_pre, dense_up_pre, up, down, combine = call(
-        own_kernel,
-        sums
-        + dense_sums
-        + [
-            out(width, hidden_units),
-            out(hidden_units, half),
-            out(tok_dev, slots, dtype=F32),
-        ],
+    gate_pre, up_pre, dense_gate_pre, dense_up_pre, combine = call(
+        functools.partial(own_kernel, high, wide),
+        sums + dense_sums + [out(tok_dev, slots, dtype=F32)],
         core,
         mine,
         gate,
-        expert_up,
-        expert_down,
+        up,
         routes.T,
         route_weight.T,
         *packs,
-        inside=(3, 4, 5, 6),
+        inside=(4, 5),
         scratch=(
             pltpu.VMEM((top, tok_dev), I32),
             pltpu.VMEM((top, tok_dev), F32),
-            dma((5,)),
+            dma((2,)),
         ),
     )
     hidden, dense_away = call(
@@ -398,21 +388,11 @@
         down,
     )
     expert_away = swap_cores(expert_away)
-    here = call(
-        here_kernel,
-        out(slots, width + lane),
-        core,
-        act,
-        hidden,
-        expert_down,
-        *packs,
-        inside=(3,),
-        scratch=(pltpu.VMEM((hidden_units, half), BF16), dma((1,))),
-    )
+    here = call(here_kernel, out(slots, width + lane), core, act, hidden, down, *packs)
     terms = call(join_kernel, out(ep_count, capacity, width + lane), here, expert_away, dense_away)
     returned = exchange(terms)
     return call(
-        functools.partial(mix_kernel, wide),
+        functools.partial(mix_kernel, high, wide),
         jax.ShapeDtypeStruct((tok_dev, half), BF16),
         returned,
         combine,

time: 79.2 us -> 80.1 us (1.011)
  blocking collectives: 26.4 us -> 61.5 us
  starting transfers between devices: 30.1 us -> 4.04 us
  Pallas kernels: 11.7 us -> 5.37 us
  waiting for transfers between devices: 10.1 us -> 8.84 us
    all_to_all x1 -> x2, blocking collectives: 26.4 us -> 61.5 us  [exchange(): lax.all_to_all(rows, EP[::-1], split_axis=0, concat_axis=0, tiled=True)]
    all_to_all x1 -> x0, starting transfers between devices: 24.2 us -> none  [exchange(): return lax.all_to_all(rows, EP, split_axis=0, concat_axis=0, tiled=True)]
    all_to_all x1 -> x0, waiting for transfers between devices: 10.1 us -> none  [exchange(): return lax.all_to_all(rows, EP, split_axis=0, concat_axis=0, tiled=True)]
    ppermute x3, waiting for transfers between devices: 0.01 us -> 8.15 us  [from_partner(): return lax.ppermute(value, EP, pairs)]
    pallas_call x7, Pallas kernels: 11.7 us -> 5.37 us  [call(): pl.pallas_call(kernel, out_shape=outs, in_specs=specs, out_specs=[spec] *...]
    ppermute x3, starting transfers between devices: 5.1 us -> 3.3 us  [from_partner(): return lax.ppermute(value, EP, pairs)]
  transfers between devices with their start and end apart: 7 -> 6, of which waited for: 1 -> 4; matrix products, arithmetic and copies ran while one was open for 0% -> 0% of each run, Pallas kernels for 9% -> 3%
where the time goes in v3:
time: 80.1 us; the launch traced here: 79.8 us
  blocking collectives  61.5 us (77%)
  waiting for transfers between devices  8.84 us (11%)
  Pallas kernels  5.37 us (7%)
  starting transfers between devices  4.04 us (5%)
    all_to_all x2, blocking collectives, exchange(): lax.all_to_all(rows, EP[::-1], split_axis=0, concat_axis=0, tiled=True)  61.5 us
    ppermute x3, waiting for transfers between devices, from_partner(): return lax.ppermute(value, EP, pairs)  8.15 us
    pallas_call x7, Pallas kernels, call(): pl.pallas_call(kernel, out_shape=outs, in_specs=specs, out_specs=[spec] *...  5.37 us
    ppermute x3, starting transfers between devices, from_partner(): return lax.ppermute(value, EP, pairs)  3.3 us
  transfers between devices with their start and end apart: 6, of which 4 were waited for; matrix products, arithmetic and copies ran while one was open for 0% of the time, Pallas kernels for 3%

profile of v3, /device:TPU:514, one launch (start us, length us, event | category | flops | bytes accessed | tf_op | source)
XLA Modules:
  0.0 79.8 jit_solution(16760543607124175837)
XLA Ops:
  0.0 0.0 copy-start.1
  0.0 0.0 copy-start.2
  0.0 1.4 %shard_map.109 = (bf16[64,2,1536]{2,1,0:T(2,128)(2,1)S(1)}, bf16[32,4736]{1,0:T(8,128)(2,1)S(1)}) custom-call(s32[1]{0:T(128)} %bitcast.core, bf16[8,1536]{1,0:T(8,128)(2,1)} %tokens_hbm.1, s32[4,8]{1,0:T(4,128)} %bitcast.7, f32[12,128]{1,0:T(8,128)} %bitcast.12, bf16[1,32]{1,0:T(2,128)(2,1)} %bitcast.13, bf16[32,1536]{1,0:T(8,128)(2,1)} %bitcast.10, ...), custom_call_target="tpu_custom_call" | custom-call | flops 99999997952 | tf_op jit(solution)/shard_map/pallas_call | solution.py:280
  1.4 36.7 %all_to_all.10.mine = bf16[64,2,1536]{2,1,0:T(2,128)(2,1)S(1)} all-to-all(bf16[64,2,1536]{2,1,0:T(2,128)(2,1)S(1)} %get-tuple-element.16), channel_id=1, replica_groups=mesh['grp'=2,'ep_0'=8,'ep_1'=8,'tp'=2] {'ep_1','ep_0'}, dimensions={0} | all-to-all | bytes 786432 | tf_op jit(solution)/shard_map/all_to_all | solution.py:314
  38.1 0.0 collective-permute-start
  38.1 0.7 collective-permute-start.3
  38.8 1.7 %collective-permute-start.2 = (bf16[32,4736]{1,0:T(8,128)(2,1)S(1)}, bf16[32,4736]{1,0:T(8,128)(2,1)S(1)}, u32[]{:S(2)}, u32[]{:S(2)}) collective-permute-start(bf16[32,4736]{1,0:T(8,128)(2,1)S(1)} %get-tuple-element.17.refs_0_), channel_id=1, source_target_pairs={{0,14},{2,4},{4,2},{6,8},{8,6},{10,12},{12,10},{14,0},{16,30},{18,... | collective-permute-start | bytes 909320 | tf_op jit(solution)/shard_map/ppermute | solution.py:56
  40.5 0.9 %collective-permute-start.1 = (bf16[32,4736]{1,0:T(8,128)(2,1)S(1)}, bf16[32,4736]{1,0:T(8,128)(2,1)S(1)}, u32[]{:S(2)}, u32[]{:S(2)}) collective-permute-start(bf16[32,4736]{1,0:T(8,128)(2,1)S(1)} %get-tuple-element.17.refs_0_), channel_id=1, source_target_pairs={{0,2},{2,0},{4,6},{6,4},{8,10},{10,8},{12,14},{14,12},{16,18},{18,... | collective-permute-start | bytes 909320 | tf_op jit(solution)/shard_map/ppermute | solution.py:56
  41.4 6.3 %collective-permute-done.3.refs_3_ = bf16[32,4736]{1,0:T(8,128)(2,1)S(1)} collective-permute-done((bf16[32,4736]{1,0:T(8,128)(2,1)S(1)}, bf16[32,4736]{1,0:T(8,128)(2,1)S(1)}, u32[]{:S(2)}, u32[]{:S(2)}) %collective-permute-start.3) | collective-permute-done | bytes 303136 | tf_op jit(solution)/shard_map/ppermute | solution.py:56
  47.7 0.4 collective-permute-done.2.refs_2_
  48.1 1.4 %collective-permute-done.1.refs_1_ = bf16[32,4736]{1,0:T(8,128)(2,1)S(1)} collective-permute-done((bf16[32,4736]{1,0:T(8,128)(2,1)S(1)}, bf16[32,4736]{1,0:T(8,128)(2,1)S(1)}, u32[]{:S(2)}, u32[]{:S(2)}) %collective-permute-start.1) | collective-permute-done | bytes 303136 | tf_op jit(solution)/shard_map/ppermute | solution.py:56
  49.5 0.0 copy-done.1
  49.5 0.0 copy-done.2
  49.5 0.0 copy-start
  49.5 1.3 %shard_map.110 = (f32[128,768]{1,0:T(8,128)S(1)}, f32[128,768]{1,0:T(8,128)S(1)}, f32[128,128]{1,0:T(8,128)S(1)}, f32[128,128]{1,0:T(8,128)S(1)}, f32[8,128]{1,0:T(8,128)S(1)}) custom-call(s32[1]{0:T(128)} %bitcast.core, bf16[64,2,1536]{2,1,0:T(2,128)(2,1)S(1)} %all_to_all.10.mine, bf16[1,1536,768]{2,1,0:T(8,128)(2,1)S(1)} %copy-done.1, ...), custom_call_target="tpu_custom_call" | custom-call | flops 1000000 | tf_op jit(solution)/shard_map/pallas_call | solution.py:280
  50.9 0.0 collective-permute-done.other
  50.9 0.5 shard_map.112
  51.4 0.1 collective-permute-start.5
  51.5 0.0 copy-done
  51.5 0.8 shard_map.111
  52.3 0.6 collective-permute-start.4
  52.9 0.4 shard_map.113.here
  53.3 0.7 collective-permute-done.4.expert_away
  54.0 0.0 collective-permute-done.5.dense_away
  54.0 0.2 shard_map.114
  54.1 24.8 %all_to_all.11.returned = bf16[64,2,1664]{2,1,0:T(2,128)(2,1)S(1)} all-to-all(bf16[64,2,1664]{2,1,0:T(2,128)(2,1)S(1)} %shard_map.114), channel_id=1, replica_groups=mesh['grp'=2,'ep_0'=8,'ep_1'=8,'tp'=2] {'ep_1','ep_0'}, dimensions={0} | all-to-all | bytes 851968 | tf_op jit(solution)/shard_map/all_to_all | solution.py:314
  78.9 0.9 %shard_map.115 = bf16[8,768]{1,0:T(8,128)(2,1)} custom-call(bf16[64,2,1664]{2,1,0:T(2,128)(2,1)S(1)} %all_to_all.11.returned, f32[8,128]{1,0:T(8,128)S(1)} %get-tuple-element.26.combine), custom_call_target="tpu_custom_call" | custom-call | flops 1000000 | tf_op jit(solution)/shard_map/pallas_call | solution.py:280
Async XLA Ops:
  0.0 49.5 %copy-start.1 = (bf16[1,1536,768]{2,1,0:T(8,128)(2,1)S(1)}, bf16[1,1536,768]{2,1,0:T(8,128)(2,1)}, u32[]{:S(2)}) copy-start(bf16[1,1536,768]{2,1,0:T(8,128)(2,1)} %gate.3) | copy-start | bytes 7077892
  0.0 49.5 %copy-start.2 = (bf16[1,1536,768]{2,1,0:T(8,128)(2,1)S(1)}, bf16[1,1536,768]{2,1,0:T(8,128)(2,1)}, u32[]{:S(2)}) copy-start(bf16[1,1536,768]{2,1,0:T(8,128)(2,1)} %up.3) | copy-start | bytes 7077892
  38.1 12.8 %collective-permute-start = (bf16[64,2,1536]{2,1,0:T(2,128)(2,1)S(1)}, bf16[64,2,1536]{2,1,0:T(2,128)(2,1)S(1)}, u32[]{:S(2)}, u32[]{:S(2)}) collective-permute-start(bf16[64,2,1536]{2,1,0:T(2,128)(2,1)S(1)} %all_to_all.10.mine), channel_id=1, source_target_pairs={{0,1},{1,0},{2,3},{3,2},{4,5},{5,4},{6,7},{7,6},{8,9},{9,8},{10,11... | collective-permute-start | bytes 1179656 | tf_op jit(solution)/shard_map/ppermute | solution.py:46
  38.1 9.6 %collective-permute-start.3 = (bf16[32,4736]{1,0:T(8,128)(2,1)S(1)}, bf16[32,4736]{1,0:T(8,128)(2,1)S(1)}, u32[]{:S(2)}, u32[]{:S(2)}) collective-permute-start(bf16[32,4736]{1,0:T(8,128)(2,1)S(1)} %get-tuple-element.17.refs_0_), channel_id=1, source_target_pairs={{0,16},{2,18},{4,20},{6,22},{8,24},{10,26},{12,28},{14,30},{16,0},... | collective-permute-start | bytes 909320 | tf_op jit(solution)/shard_map/ppermute | solution.py:56
  38.8 9.3 %collective-permute-start.2 = (bf16[32,4736]{1,0:T(8,128)(2,1)S(1)}, bf16[32,4736]{1,0:T(8,128)(2,1)S(1)}, u32[]{:S(2)}, u32[]{:S(2)}) collective-permute-start(bf16[32,4736]{1,0:T(8,128)(2,1)S(1)} %get-tuple-element.17.refs_0_), channel_id=1, source_target_pairs={{0,14},{2,4},{4,2},{6,8},{8,6},{10,12},{12,10},{14,0},{16,30},{18,... | collective-permute-start | bytes 909320 | tf_op jit(solution)/shard_map/ppermute | solution.py:56
  40.5 9.0 %collective-permute-start.1 = (bf16[32,4736]{1,0:T(8,128)(2,1)S(1)}, bf16[32,4736]{1,0:T(8,128)(2,1)S(1)}, u32[]{:S(2)}, u32[]{:S(2)}) collective-permute-start(bf16[32,4736]{1,0:T(8,128)(2,1)S(1)} %get-tuple-element.17.refs_0_), channel_id=1, source_target_pairs={{0,2},{2,0},{4,6},{6,4},{8,10},{10,8},{12,14},{14,12},{16,18},{18,... | collective-permute-start | bytes 909320 | tf_op jit(solution)/shard_map/ppermute | solution.py:56
  49.5 2.0 %copy-start = (bf16[1,768,1536]{2,1,0:T(8,128)(2,1)S(1)}, bf16[1,768,1536]{2,1,0:T(8,128)(2,1)}, u32[]{:S(2)}) copy-start(bf16[1,768,1536]{2,1,0:T(8,128)(2,1)} %down.3) | copy-start | bytes 7077892
  51.4 2.6 %collective-permute-start.5 = (bf16[128,896]{1,0:T(8,128)(2,1)S(1)}, bf16[128,896]{1,0:T(8,128)(2,1)S(1)}, u32[]{:S(2)}, u32[]{:S(2)}) collective-permute-start(bf16[128,896]{1,0:T(8,128)(2,1)S(1)} %get-tuple-element.25), channel_id=1, source_target_pairs={{0,1},{1,0},{2,3},{3,2},{4,5},{5,4},{6,7},{7,6},{8,9},{9,8},{10,11... | collective-permute-start | bytes 688136 | tf_op jit(solution)/shard_map/ppermute | solution.py:46
  52.3 1.7 %collective-permute-start.4 = (bf16[128,768]{1,0:T(8,128)(2,1)S(1)}, bf16[128,768]{1,0:T(8,128)(2,1)S(1)}, u32[]{:S(2)}, u32[]{:S(2)}) collective-permute-start(bf16[128,768]{1,0:T(8,128)(2,1)S(1)} %get-tuple-element.24), channel_id=1, source_target_pairs={{0,1},{1,0},{2,3},{3,2},{4,5},{5,4},{6,7},{7,6},{8,9},{9,8},{10,11... | collective-permute-start | bytes 589832 | tf_op jit(solution)/shard_map/ppermute | solution.py:46

commit v4 on v3

--- a/solution.py
+++ b/solution.py
@@ -57,9 +57,9 @@
 
 
 partners = (
-    lambda y, x: (y, x ^ 1),
-    lambda y, x: (y, ((x + 1) ^ 1) - 1),
-    lambda y, x: (y ^ 1, x),
+    lambda y, x: (y, x + 1),
+    lambda y, x: (y + 1, x),
+    lambda y, x: (y, x - 1),
 )
 
 
@@ -258,8 +258,10 @@
     rest = combine[...] - first.astype(F32)
     second = rest.astype(BF16)
     third = (rest - second.astype(F32)).astype(BF16)
-    expert_rows = returned[:, :, :half].reshape(slots, half)
-    expert_mix = dot(first, expert_rows) + (dot(second, expert_rows) + dot(third, expert_rows))
+    terms = [first.astype(F32), second.astype(F32), third.astype(F32)]
+    stacked = jnp.concatenate(terms, axis=0).astype(BF16)
+    parts = dot(stacked, returned[:, :, :half].reshape(slots, half))
+    expert_mix = parts[:tok_dev] + (parts[tok_dev : 2 * tok_dev] + parts[2 * tok_dev :])
     out[...] = (jax.nn.sigmoid(gate_logit) * dense_out + expert_mix).astype(BF16)
 
 

time: 80.1 us -> 82.2 us (1.026)
  waiting for transfers between devices: 8.84 us -> 10.3 us
  blocking collectives: 61.5 us -> 62.7 us
    ppermute x3, waiting for transfers between devices: 8.15 us -> 9.62 us  [from_partner(): return lax.ppermute(value, EP, pairs)]
    all_to_all x2, blocking collectives: 61.5 us -> 62.7 us  [exchange(): lax.all_to_all(rows, EP[::-1], split_axis=0, concat_axis=0, tiled=True)]
  transfers between devices with their start and end apart: 6 -> 6, of which waited for: 4 -> 3; matrix products, arithmetic and copies ran while one was open for 0% -> 0% of each run, Pallas kernels for 3% -> 3%
where the time goes in v4:
time: 82.2 us; the launch traced here: 81.9 us
  blocking collectives  62.7 us (76%)
  waiting for transfers between devices  10.3 us (13%)
  Pallas kernels  5.36 us (7%)
  starting transfers between devices  3.48 us (4%)
    all_to_all x2, blocking collectives, exchange(): lax.all_to_all(rows, EP[::-1], split_axis=0, concat_axis=0, tiled=True)  62.7 us
    ppermute x3, waiting for transfers between devices, from_partner(): return lax.ppermute(value, EP, pairs)  9.62 us
    pallas_call x7, Pallas kernels, call(): pl.pallas_call(kernel, out_shape=outs, in_specs=specs, out_specs=[spec] *...  5.36 us
    ppermute x3, starting transfers between devices, from_partner(): return lax.ppermute(value, EP, pairs)  2.75 us
  transfers between devices with their start and end apart: 6, of which 3 were waited for; matrix products, arithmetic and copies ran while one was open for 0% of the time, Pallas kernels for 3%

profile of v4, /device:TPU:514, one launch (start us, length us, event | category | flops | bytes accessed | tf_op | source)
XLA Modules:
  0.0 81.9 jit_solution(12285251913914372714)
XLA Ops:
  0.0 0.0 copy-start.1
  0.0 0.0 copy-start.2
  0.0 1.4 %shard_map.109 = (bf16[64,2,1536]{2,1,0:T(2,128)(2,1)S(1)}, bf16[32,4736]{1,0:T(8,128)(2,1)S(1)}) custom-call(s32[1]{0:T(128)} %bitcast.core, bf16[8,1536]{1,0:T(8,128)(2,1)} %tokens_hbm.1, s32[4,8]{1,0:T(4,128)} %bitcast.7, f32[12,128]{1,0:T(8,128)} %bitcast.12, bf16[1,32]{1,0:T(2,128)(2,1)} %bitcast.13, bf16[32,1536]{1,0:T(8,128)(2,1)} %bitcast.10, ...), custom_call_target="tpu_custom_call" | custom-call | flops 99999997952 | tf_op jit(solution)/shard_map/pallas_call | solution.py:282
  1.4 36.7 %all_to_all.10.mine = bf16[64,2,1536]{2,1,0:T(2,128)(2,1)S(1)} all-to-all(bf16[64,2,1536]{2,1,0:T(2,128)(2,1)S(1)} %get-tuple-element.16), channel_id=1, replica_groups=mesh['grp'=2,'ep_0'=8,'ep_1'=8,'tp'=2] {'ep_1','ep_0'}, dimensions={0} | all-to-all | bytes 786432 | tf_op jit(solution)/shard_map/all_to_all | solution.py:316
  38.1 0.0 collective-permute-start
  38.1 1.8 %collective-permute-start.3 = (bf16[32,4736]{1,0:T(8,128)(2,1)S(1)}, bf16[32,4736]{1,0:T(8,128)(2,1)S(1)}, u32[]{:S(2)}, u32[]{:S(2)}) collective-permute-start(bf16[32,4736]{1,0:T(8,128)(2,1)S(1)} %get-tuple-element.17.refs_0_), channel_id=1, source_target_pairs={{0,14},{2,0},{4,2},{6,4},{8,6},{10,8},{12,10},{14,12},{16,30},{18,... | collective-permute-start | bytes 909320 | tf_op jit(solution)/shard_map/ppermute | solution.py:56
  39.9 0.9 %collective-permute-start.2 = (bf16[32,4736]{1,0:T(8,128)(2,1)S(1)}, bf16[32,4736]{1,0:T(8,128)(2,1)S(1)}, u32[]{:S(2)}, u32[]{:S(2)}) collective-permute-start(bf16[32,4736]{1,0:T(8,128)(2,1)S(1)} %get-tuple-element.17.refs_0_), channel_id=1, source_target_pairs={{0,16},{2,18},{4,20},{6,22},{8,24},{10,26},{12,28},{14,30},{16,32}... | collective-permute-start | bytes 909320 | tf_op jit(solution)/shard_map/ppermute | solution.py:56
  40.8 0.0 collective-permute-start.1
  40.8 6.8 %collective-permute-done.3.refs_3_ = bf16[32,4736]{1,0:T(8,128)(2,1)S(1)} collective-permute-done((bf16[32,4736]{1,0:T(8,128)(2,1)S(1)}, bf16[32,4736]{1,0:T(8,128)(2,1)S(1)}, u32[]{:S(2)}, u32[]{:S(2)}) %collective-permute-start.3) | collective-permute-done | bytes 303136 | tf_op jit(solution)/shard_map/ppermute | solution.py:56
  47.7 2.8 %collective-permute-done.2.refs_2_ = bf16[32,4736]{1,0:T(8,128)(2,1)S(1)} collective-permute-done((bf16[32,4736]{1,0:T(8,128)(2,1)S(1)}, bf16[32,4736]{1,0:T(8,128)(2,1)S(1)}, u32[]{:S(2)}, u32[]{:S(2)}) %collective-permute-start.2) | collective-permute-done | bytes 303136 | tf_op jit(solution)/shard_map/ppermute | solution.py:56
  50.4 0.0 collective-permute-done.1.refs_1_
  50.4 0.0 copy-done.1
  50.5 0.0 copy-done.2
  50.5 0.0 copy-start
  50.5 1.3 %shard_map.110 = (f32[128,768]{1,0:T(8,128)S(1)}, f32[128,768]{1,0:T(8,128)S(1)}, f32[128,128]{1,0:T(8,128)S(1)}, f32[128,128]{1,0:T(8,128)S(1)}, f32[8,128]{1,0:T(8,128)S(1)}) custom-call(s32[1]{0:T(128)} %bitcast.core, bf16[64,2,1536]{2,1,0:T(2,128)(2,1)S(1)} %all_to_all.10.mine, bf16[1,1536,768]{2,1,0:T(8,128)(2,1)S(1)} %copy-done.1, ...), custom_call_target="tpu_custom_call" | custom-call | flops 1000000 | tf_op jit(solution)/shard_map/pallas_call | solution.py:282
  51.8 0.0 collective-permute-done.other
  51.8 0.5 shard_map.112
  52.3 0.1 collective-permute-start.5
  52.4 0.0 copy-done
  52.4 0.8 shard_map.111
  53.2 0.6 collective-permute-start.4
  53.8 0.4 shard_map.113.here
  54.2 0.7 collective-permute-done.4.expert_away
  54.9 0.0 collective-permute-done.5.dense_away
  54.9 0.2 shard_map.114
  55.1 26.0 %all_to_all.11.returned = bf16[64,2,1664]{2,1,0:T(2,128)(2,1)S(1)} all-to-all(bf16[64,2,1664]{2,1,0:T(2,128)(2,1)S(1)} %shard_map.114), channel_id=1, replica_groups=mesh['grp'=2,'ep_0'=8,'ep_1'=8,'tp'=2] {'ep_1','ep_0'}, dimensions={0} | all-to-all | bytes 851968 | tf_op jit(solution)/shard_map/all_to_all | solution.py:316
  81.1 0.9 %shard_map.115 = bf16[8,768]{1,0:T(8,128)(2,1)} custom-call(bf16[64,2,1664]{2,1,0:T(2,128)(2,1)S(1)} %all_to_all.11.returned, f32[8,128]{1,0:T(8,128)S(1)} %get-tuple-element.26.combine), custom_call_target="tpu_custom_call" | custom-call | flops 1000000 | tf_op jit(solution)/shard_map/pallas_call | solution.py:282
Async XLA Ops:
  0.0 50.4 %copy-start.1 = (bf16[1,1536,768]{2,1,0:T(8,128)(2,1)S(1)}, bf16[1,1536,768]{2,1,0:T(8,128)(2,1)}, u32[]{:S(2)}) copy-start(bf16[1,1536,768]{2,1,0:T(8,128)(2,1)} %gate.3) | copy-start | bytes 7077892
  0.0 50.5 %copy-start.2 = (bf16[1,1536,768]{2,1,0:T(8,128)(2,1)S(1)}, bf16[1,1536,768]{2,1,0:T(8,128)(2,1)}, u32[]{:S(2)}) copy-start(bf16[1,1536,768]{2,1,0:T(8,128)(2,1)} %up.3) | copy-start | bytes 7077892
  38.1 13.7 %collective-permute-start = (bf16[64,2,1536]{2,1,0:T(2,128)(2,1)S(1)}, bf16[64,2,1536]{2,1,0:T(2,128)(2,1)S(1)}, u32[]{:S(2)}, u32[]{:S(2)}) collective-permute-start(bf16[64,2,1536]{2,1,0:T(2,128)(2,1)S(1)} %all_to_all.10.mine), channel_id=1, source_target_pairs={{0,1},{1,0},{2,3},{3,2},{4,5},{5,4},{6,7},{7,6},{8,9},{9,8},{10,11... | collective-permute-start | bytes 1179656 | tf_op jit(solution)/shard_map/ppermute | solution.py:46
  38.1 9.6 %collective-permute-start.3 = (bf16[32,4736]{1,0:T(8,128)(2,1)S(1)}, bf16[32,4736]{1,0:T(8,128)(2,1)S(1)}, u32[]{:S(2)}, u32[]{:S(2)}) collective-permute-start(bf16[32,4736]{1,0:T(8,128)(2,1)S(1)} %get-tuple-element.17.refs_0_), channel_id=1, source_target_pairs={{0,14},{2,0},{4,2},{6,4},{8,6},{10,8},{12,10},{14,12},{16,30},{18,... | collective-permute-start | bytes 909320 | tf_op jit(solution)/shard_map/ppermute | solution.py:56
  39.9 10.5 %collective-permute-start.2 = (bf16[32,4736]{1,0:T(8,128)(2,1)S(1)}, bf16[32,4736]{1,0:T(8,128)(2,1)S(1)}, u32[]{:S(2)}, u32[]{:S(2)}) collective-permute-start(bf16[32,4736]{1,0:T(8,128)(2,1)S(1)} %get-tuple-element.17.refs_0_), channel_id=1, source_target_pairs={{0,16},{2,18},{4,20},{6,22},{8,24},{10,26},{12,28},{14,30},{16,32}... | collective-permute-start | bytes 909320 | tf_op jit(solution)/shard_map/ppermute | solution.py:56
  40.8 9.6 %collective-permute-start.1 = (bf16[32,4736]{1,0:T(8,128)(2,1)S(1)}, bf16[32,4736]{1,0:T(8,128)(2,1)S(1)}, u32[]{:S(2)}, u32[]{:S(2)}) collective-permute-start(bf16[32,4736]{1,0:T(8,128)(2,1)S(1)} %get-tuple-element.17.refs_0_), channel_id=1, source_target_pairs={{0,2},{2,4},{4,6},{6,8},{8,10},{10,12},{12,14},{14,0},{16,18},{18,... | collective-permute-start | bytes 909320 | tf_op jit(solution)/shard_map/ppermute | solution.py:56
  50.5 2.0 %copy-start = (bf16[1,768,1536]{2,1,0:T(8,128)(2,1)S(1)}, bf16[1,768,1536]{2,1,0:T(8,128)(2,1)}, u32[]{:S(2)}) copy-start(bf16[1,768,1536]{2,1,0:T(8,128)(2,1)} %down.3) | copy-start | bytes 7077892
  52.3 2.6 %collective-permute-start.5 = (bf16[128,896]{1,0:T(8,128)(2,1)S(1)}, bf16[128,896]{1,0:T(8,128)(2,1)S(1)}, u32[]{:S(2)}, u32[]{:S(2)}) collective-permute-start(bf16[128,896]{1,0:T(8,128)(2,1)S(1)} %get-tuple-element.25), channel_id=1, source_target_pairs={{0,1},{1,0},{2,3},{3,2},{4,5},{5,4},{6,7},{7,6},{8,9},{9,8},{10,11... | collective-permute-start | bytes 688136 | tf_op jit(solution)/shard_map/ppermute | solution.py:46
  53.2 1.7 %collective-permute-start.4 = (bf16[128,768]{1,0:T(8,128)(2,1)S(1)}, bf16[128,768]{1,0:T(8,128)(2,1)S(1)}, u32[]{:S(2)}, u32[]{:S(2)}) collective-permute-start(bf16[128,768]{1,0:T(8,128)(2,1)S(1)} %get-tuple-element.24), channel_id=1, source_target_pairs={{0,1},{1,0},{2,3},{3,2},{4,5},{5,4},{6,7},{7,6},{8,9},{9,8},{10,11... | collective-permute-start | bytes 589832 | tf_op jit(solution)/shard_map/ppermute | solution.py:46

commit v5 on v3

--- a/solution.py
+++ b/solution.py
@@ -143,8 +143,9 @@
     normed = jnp.concatenate(normed, axis=1)
     spread = jnp.where(same, vector[...].astype(F32), 0.0).astype(BF16)
     pack[:, 3 * width :] = dot(spread, lead).astype(BF16)
-    out[:, :, :half] = dot(taken, normed).astype(BF16).reshape(ep_count, capacity, half)
-    out[:, :, half:] = dot(wanted, normed).astype(BF16).reshape(ep_count, capacity, half)
+    picked = dot(jnp.concatenate([taken, wanted], axis=0), normed).astype(BF16)
+    out[:, :, :half] = picked[:slots].reshape(ep_count, capacity, half)
+    out[:, :, half:] = picked[slots:].reshape(ep_count, capacity, half)
     for copy in copies[4:]:
         copy.wait()
 

time: 80.1 us -> 80.1 us (level)
  no operation moved by 1% of the time
where the time goes in v5:
time: 80.1 us; the launch traced here: 79.8 us
  blocking collectives  61.5 us (77%)
  waiting for transfers between devices  8.84 us (11%)
  Pallas kernels  5.37 us (7%)
  starting transfers between devices  4.04 us (5%)
    all_to_all x2, blocking collectives, exchange(): lax.all_to_all(rows, EP[::-1], split_axis=0, concat_axis=0, tiled=True)  61.5 us
    ppermute x3, waiting for transfers between devices, from_partner(): return lax.ppermute(value, EP, pairs)  8.15 us
    pallas_call x7, Pallas kernels, call(): pl.pallas_call(kernel, out_shape=outs, in_specs=specs, out_specs=[spec] *...  5.37 us
    ppermute x3, starting transfers between devices, from_partner(): return lax.ppermute(value, EP, pairs)  3.3 us
  transfers between devices with their start and end apart: 6, of which 4 were waited for; matrix products, arithmetic and copies ran while one was open for 0% of the time, Pallas kernels for 3%

profile of v5, /device:TPU:514, one launch (start us, length us, event | category | flops | bytes accessed | tf_op | source)
XLA Modules:
  0.0 79.8 jit_solution(17958142327497361939)
XLA Ops:
  0.0 0.0 copy-start.1
  0.0 0.0 copy-start.2
  0.0 1.4 %shard_map.109 = (bf16[64,2,1536]{2,1,0:T(2,128)(2,1)S(1)}, bf16[32,4736]{1,0:T(8,128)(2,1)S(1)}) custom-call(s32[1]{0:T(128)} %bitcast.core, bf16[8,1536]{1,0:T(8,128)(2,1)} %tokens_hbm.1, s32[4,8]{1,0:T(4,128)} %bitcast.7, f32[12,128]{1,0:T(8,128)} %bitcast.12, bf16[1,32]{1,0:T(2,128)(2,1)} %bitcast.13, bf16[32,1536]{1,0:T(8,128)(2,1)} %bitcast.10, ...), custom_call_target="tpu_custom_call" | custom-call | flops 99999997952 | tf_op jit(solution)/shard_map/pallas_call | solution.py:281
  1.4 36.7 %all_to_all.10.mine = bf16[64,2,1536]{2,1,0:T(2,128)(2,1)S(1)} all-to-all(bf16[64,2,1536]{2,1,0:T(2,128)(2,1)S(1)} %get-tuple-element.16), channel_id=1, replica_groups=mesh['grp'=2,'ep_0'=8,'ep_1'=8,'tp'=2] {'ep_1','ep_0'}, dimensions={0} | all-to-all | bytes 786432 | tf_op jit(solution)/shard_map/all_to_all | solution.py:315
  38.1 0.0 collective-permute-start
  38.1 0.7 collective-permute-start.3
  38.8 1.7 %collective-permute-start.2 = (bf16[32,4736]{1,0:T(8,128)(2,1)S(1)}, bf16[32,4736]{1,0:T(8,128)(2,1)S(1)}, u32[]{:S(2)}, u32[]{:S(2)}) collective-permute-start(bf16[32,4736]{1,0:T(8,128)(2,1)S(1)} %get-tuple-element.17.refs_0_), channel_id=1, source_target_pairs={{0,14},{2,4},{4,2},{6,8},{8,6},{10,12},{12,10},{14,0},{16,30},{18,... | collective-permute-start | bytes 909320 | tf_op jit(solution)/shard_map/ppermute | solution.py:56
  40.5 0.9 %collective-permute-start.1 = (bf16[32,4736]{1,0:T(8,128)(2,1)S(1)}, bf16[32,4736]{1,0:T(8,128)(2,1)S(1)}, u32[]{:S(2)}, u32[]{:S(2)}) collective-permute-start(bf16[32,4736]{1,0:T(8,128)(2,1)S(1)} %get-tuple-element.17.refs_0_), channel_id=1, source_target_pairs={{0,2},{2,0},{4,6},{6,4},{8,10},{10,8},{12,14},{14,12},{16,18},{18,... | collective-permute-start | bytes 909320 | tf_op jit(solution)/shard_map/ppermute | solution.py:56
  41.4 6.3 %collective-permute-done.3.refs_3_ = bf16[32,4736]{1,0:T(8,128)(2,1)S(1)} collective-permute-done((bf16[32,4736]{1,0:T(8,128)(2,1)S(1)}, bf16[32,4736]{1,0:T(8,128)(2,1)S(1)}, u32[]{:S(2)}, u32[]{:S(2)}) %collective-permute-start.3) | collective-permute-done | bytes 303136 | tf_op jit(solution)/shard_map/ppermute | solution.py:56
  47.7 0.4 collective-permute-done.2.refs_2_
  48.1 1.4 %collective-permute-done.1.refs_1_ = bf16[32,4736]{1,0:T(8,128)(2,1)S(1)} collective-permute-done((bf16[32,4736]{1,0:T(8,128)(2,1)S(1)}, bf16[32,4736]{1,0:T(8,128)(2,1)S(1)}, u32[]{:S(2)}, u32[]{:S(2)}) %collective-permute-start.1) | collective-permute-done | bytes 303136 | tf_op jit(solution)/shard_map/ppermute | solution.py:56
  49.5 0.0 copy-done.1
  49.5 0.0 copy-done.2
  49.5 0.0 copy-start
  49.6 1.3 %shard_map.110 = (f32[128,768]{1,0:T(8,128)S(1)}, f32[128,768]{1,0:T(8,128)S(1)}, f32[128,128]{1,0:T(8,128)S(1)}, f32[128,128]{1,0:T(8,128)S(1)}, f32[8,128]{1,0:T(8,128)S(1)}) custom-call(s32[1]{0:T(128)} %bitcast.core, bf16[64,2,1536]{2,1,0:T(2,128)(2,1)S(1)} %all_to_all.10.mine, bf16[1,1536,768]{2,1,0:T(8,128)(2,1)S(1)} %copy-done.1, ...), custom_call_target="tpu_custom_call" | custom-call | flops 1000000 | tf_op jit(solution)/shard_map/pallas_call | solution.py:281
  50.9 0.0 collective-permute-done.other
  50.9 0.5 shard_map.112
  51.4 0.1 collective-permute-start.5
  51.5 0.0 copy-done
  51.5 0.8 shard_map.111
  52.3 0.6 collective-permute-start.4
  52.9 0.4 shard_map.113.here
  53.3 0.7 collective-permute-done.4.expert_away
  54.0 0.0 collective-permute-done.5.dense_away
  54.0 0.2 shard_map.114
  54.1 24.8 %all_to_all.11.returned = bf16[64,2,1664]{2,1,0:T(2,128)(2,1)S(1)} all-to-all(bf16[64,2,1664]{2,1,0:T(2,128)(2,1)S(1)} %shard_map.114), channel_id=1, replica_groups=mesh['grp'=2,'ep_0'=8,'ep_1'=8,'tp'=2] {'ep_1','ep_0'}, dimensions={0} | all-to-all | bytes 851968 | tf_op jit(solution)/shard_map/all_to_all | solution.py:315
  78.9 0.9 %shard_map.115 = bf16[8,768]{1,0:T(8,128)(2,1)} custom-call(bf16[64,2,1664]{2,1,0:T(2,128)(2,1)S(1)} %all_to_all.11.returned, f32[8,128]{1,0:T(8,128)S(1)} %get-tuple-element.26.combine), custom_call_target="tpu_custom_call" | custom-call | flops 1000000 | tf_op jit(solution)/shard_map/pallas_call | solution.py:281
Async XLA Ops:
  0.0 49.5 %copy-start.1 = (bf16[1,1536,768]{2,1,0:T(8,128)(2,1)S(1)}, bf16[1,1536,768]{2,1,0:T(8,128)(2,1)}, u32[]{:S(2)}) copy-start(bf16[1,1536,768]{2,1,0:T(8,128)(2,1)} %gate.3) | copy-start | bytes 7077892
  0.0 49.5 %copy-start.2 = (bf16[1,1536,768]{2,1,0:T(8,128)(2,1)S(1)}, bf16[1,1536,768]{2,1,0:T(8,128)(2,1)}, u32[]{:S(2)}) copy-start(bf16[1,1536,768]{2,1,0:T(8,128)(2,1)} %up.3) | copy-start | bytes 7077892
  38.1 12.8 %collective-permute-start = (bf16[64,2,1536]{2,1,0:T(2,128)(2,1)S(1)}, bf16[64,2,1536]{2,1,0:T(2,128)(2,1)S(1)}, u32[]{:S(2)}, u32[]{:S(2)}) collective-permute-start(bf16[64,2,1536]{2,1,0:T(2,128)(2,1)S(1)} %all_to_all.10.mine), channel_id=1, source_target_pairs={{0,1},{1,0},{2,3},{3,2},{4,5},{5,4},{6,7},{7,6},{8,9},{9,8},{10,11... | collective-permute-start | bytes 1179656 | tf_op jit(solution)/shard_map/ppermute | solution.py:46
  38.1 9.6 %collective-permute-start.3 = (bf16[32,4736]{1,0:T(8,128)(2,1)S(1)}, bf16[32,4736]{1,0:T(8,128)(2,1)S(1)}, u32[]{:S(2)}, u32[]{:S(2)}) collective-permute-start(bf16[32,4736]{1,0:T(8,128)(2,1)S(1)} %get-tuple-element.17.refs_0_), channel_id=1, source_target_pairs={{0,16},{2,18},{4,20},{6,22},{8,24},{10,26},{12,28},{14,30},{16,0},... | collective-permute-start | bytes 909320 | tf_op jit(solution)/shard_map/ppermute | solution.py:56
  38.8 9.3 %collective-permute-start.2 = (bf16[32,4736]{1,0:T(8,128)(2,1)S(1)}, bf16[32,4736]{1,0:T(8,128)(2,1)S(1)}, u32[]{:S(2)}, u32[]{:S(2)}) collective-permute-start(bf16[32,4736]{1,0:T(8,128)(2,1)S(1)} %get-tuple-element.17.refs_0_), channel_id=1, source_target_pairs={{0,14},{2,4},{4,2},{6,8},{8,6},{10,12},{12,10},{14,0},{16,30},{18,... | collective-permute-start | bytes 909320 | tf_op jit(solution)/shard_map/ppermute | solution.py:56
  40.5 9.0 %collective-permute-start.1 = (bf16[32,4736]{1,0:T(8,128)(2,1)S(1)}, bf16[32,4736]{1,0:T(8,128)(2,1)S(1)}, u32[]{:S(2)}, u32[]{:S(2)}) collective-permute-start(bf16[32,4736]{1,0:T(8,128)(2,1)S(1)} %get-tuple-element.17.refs_0_), channel_id=1, source_target_pairs={{0,2},{2,0},{4,6},{6,4},{8,10},{10,8},{12,14},{14,12},{16,18},{18,... | collective-permute-start | bytes 909320 | tf_op jit(solution)/shard_map/ppermute | solution.py:56
  49.5 2.0 %copy-start = (bf16[1,768,1536]{2,1,0:T(8,128)(2,1)S(1)}, bf16[1,768,1536]{2,1,0:T(8,128)(2,1)}, u32[]{:S(2)}) copy-start(bf16[1,768,1536]{2,1,0:T(8,128)(2,1)} %down.3) | copy-start | bytes 7077892
  51.4 2.6 %collective-permute-start.5 = (bf16[128,896]{1,0:T(8,128)(2,1)S(1)}, bf16[128,896]{1,0:T(8,128)(2,1)S(1)}, u32[]{:S(2)}, u32[]{:S(2)}) collective-permute-start(bf16[128,896]{1,0:T(8,128)(2,1)S(1)} %get-tuple-element.25), channel_id=1, source_target_pairs={{0,1},{1,0},{2,3},{3,2},{4,5},{5,4},{6,7},{7,6},{8,9},{9,8},{10,11... | collective-permute-start | bytes 688136 | tf_op jit(solution)/shard_map/ppermute | solution.py:46
  52.3 1.7 %collective-permute-start.4 = (bf16[128,768]{1,0:T(8,128)(2,1)S(1)}, bf16[128,768]{1,0:T(8,128)(2,1)S(1)}, u32[]{:S(2)}, u32[]{:S(2)}) collective-permute-start(bf16[128,768]{1,0:T(8,128)(2,1)S(1)} %get-tuple-element.24), channel_id=1, source_target_pairs={{0,1},{1,0},{2,3},{3,2},{4,5},{5,4},{6,7},{7,6},{8,9},{9,8},{10,11... | collective-permute-start | bytes 589832 | tf_op jit(solution)/shard_map/ppermute | solution.py:46
